TPU v7x, 32 devices: a whole 2x2x4 slice. The times are simulated.
32 devices in a mesh: sp: 4 (over z), fs: 4 (over y, x), tp: 2 (over core).
Axes of the slice: x: 2, y: 2, z: 4, core: 2. Of those that a mesh axis runs over, the one named last changes fastest.
Arguments:
- tokens: bfloat16 [4, 512, 2048], P('fs', ('sp', 'tp')), may hold values from -6 to 6
- input_norm_gain: float32 [2048], replicated, may hold values from 0.1 to 1.9
- pooling_input_weight: bfloat16 [2048, 1024], P('sp', 'tp'), may hold values from -0.125 to 0.125
- query_weight: bfloat16 [2048, 1024], P('sp', 'tp'), may hold values from -0.125 to 0.125
- forget_weight: bfloat16 [2048, 1024], P('sp', 'tp'), may hold values from -0.125 to 0.125
- value_weight: bfloat16 [2048, 1024], P('sp', 'tp'), may hold values from -0.125 to 0.125
- pooling_group_maps: bfloat16 [4, 256, 256], P('tp'), may hold values from -0.375 to 0.375
- pooling_scale: float32 [1024], P('tp'), may hold values from 0.1 to 1.9
- lower_bound_logits: float32 [1024], P('tp')
- decay_spike: float32 [4, 512, 8], P('fs', 'sp', 'tp'), may hold values from -0.75 to 0
- head_norm_gain: float32 [1024], P('tp'), may hold values from 0.1 to 1.9
- pooling_output_weight: bfloat16 [1024, 2048], P('tp', 'sp'), may hold values from -0.125 to 0.125
- recurrent_output_weight: bfloat16 [1024, 2048], P('tp', 'sp'), may hold values from -0.125 to 0.125
Outputs:
- mixed: bfloat16 [4, 512, 2048], P('fs', ('sp', 'tp'))
All inputs are finite; a program needn't handle non-finite values.
Results may differ from a plain program's by a relative error of at most 0.013.
Values may be sent and summed in bfloat16 or wider, within the bound.
A program may use at most 64 MiB of HBM per device.

v0:
```python
import functools

import jax
import jax.numpy as jnp
from jax import lax
from jax.experimental import pallas as pl
from jax.experimental.pallas import tpu as pltpu
from jax.sharding import PartitionSpec as P

BLOCK = 64


EPSILON = 1e-06
HIGHEST = lax.Precision.HIGHEST


def shifted(value, axis, steps):
    count = lax.axis_size(axis)
    first, last = (max(0, -steps), min(count, count - steps))
    return lax.ppermute(value, axis, [(source, source + steps) for source in range(first, last)])


def entering(shard, axis, join, neutral):
    place = lax.axis_index(axis)
    gathered = jax.tree.map(
        lambda a, kind: lax.all_gather(a.astype(kind), axis), shard, (jnp.bfloat16, jnp.bfloat16)
    )
    state = jax.tree.map(lambda a, e: jnp.zeros_like(a) + jnp.asarray(e, a.dtype), shard, neutral)

    def one(step, state):
        return join(
            state,
            jax.tree.map(
                lambda a, own: lax.dynamic_index_in_dim(a, step, 0, False).astype(own.dtype),
                gathered,
                shard,
            ),
        )

    return lax.fori_loop(0, place, one, state)


def rms_scale(values, gain):
    return values * lax.rsqrt(jnp.mean(values * values, axis=-1, keepdims=True) + EPSILON) * gain


def join_state(earlier, later):
    decay_one, state_one = earlier
    decay_two, state_two = later
    return (decay_one * decay_two, decay_two[..., None] * state_one + state_two)


def body(
    tokens,
    input_norm_gain,
    pooling_input_weight,
    query_weight,
    forget_weight,
    value_weight,
    pooling_group_maps,
    pooling_scale,
    lower_bound_logits,
    decay_spike,
    head_norm_gain,
    pooling_output_weight,
    recurrent_output_weight,
):
    gathered = lax.all_gather(tokens, "tp", axis=1, tiled=True)[0]
    length_total = gathered.shape[0]
    normed = rms_scale(gathered.astype(jnp.float32), input_norm_gain).astype(jnp.bfloat16)
    pool_width = pooling_input_weight.shape[1]
    rec_width = query_weight.shape[1]
    stacked = jnp.concatenate(
        [pooling_input_weight, query_weight, forget_weight, value_weight], axis=1
    )
    out_local = jnp.concatenate([pooling_output_weight, recurrent_output_weight], axis=0)
    groups_fs = lax.axis_size("fs")
    member = lax.axis_index("fs")
    slice_width = stacked.shape[1] // groups_fs
    own_slice = lax.dynamic_slice_in_dim(stacked, member * slice_width, slice_width, 1)
    column_part = lax.all_gather(own_slice, "sp", axis=0, tiled=True)
    full_input = lax.all_gather(column_part, "fs", axis=1, tiled=True)
    projected = jnp.dot(normed, full_input, preferred_element_type=jnp.float32)
    slice_height = out_local.shape[0] // groups_fs
    own_rows = lax.dynamic_slice_in_dim(out_local, member * slice_height, slice_height, 0)
    row_part = lax.all_gather(own_rows, "sp", axis=1, tiled=True)
    out_full = lax.all_gather(row_part, "fs", axis=0, tiled=True)
    rounded = lax.optimization_barrier(projected.astype(jnp.bfloat16))
    pool_input = rounded[:, :pool_width]
    query_matrix = rounded[:, pool_width : pool_width + rec_width].astype(jnp.float32)
    forget_gate_logit = rounded[:, pool_width + rec_width : pool_width + 2 * rec_width].astype(
        jnp.float32
    )
    value_projected = rounded[:, pool_width + 2 * rec_width :].astype(jnp.float32)
    groups_local = pooling_group_maps.shape[0]
    group_size = pooling_group_maps.shape[1]
    reach_rows = 2 ** (groups_local * lax.axis_size("tp"))
    previous = shifted(pool_input[length_total - reach_rows :], "sp", 1)
    extended = jnp.concatenate([previous, pool_input], axis=0).astype(jnp.float32)
    extended = extended.reshape(reach_rows + length_total, groups_local, group_size)
    group_ids = lax.axis_index("tp") * groups_local + jnp.arange(groups_local, dtype=jnp.int32)
    windows = jnp.left_shift(jnp.int32(2), group_ids)
    window_sum = jnp.zeros((length_total, groups_local, group_size), jnp.float32)
    for offset in range(reach_rows):
        inside = (offset < windows).astype(jnp.float32)
        window_sum = (
            window_sum
            + extended[reach_rows - offset : reach_rows - offset + length_total] * inside[:, None]
        )
    position_index = lax.axis_index("sp") * length_total + jnp.arange(length_total, dtype=jnp.int32)
    counts = jnp.minimum(position_index[:, None] + 1, windows[None, :]).astype(jnp.float32)
    pool_diff = (window_sum / counts[:, :, None] - extended[reach_rows:]).astype(jnp.bfloat16)
    pool_mapped = jnp.einsum(
        "tgc,gcd->tgd", pool_diff, pooling_group_maps, preferred_element_type=jnp.float32
    )
    pool_out = (pool_mapped.reshape(length_total, pool_width) * pooling_scale).astype(jnp.bfloat16)
    local_heads = decay_spike.shape[2]
    head_width = rec_width // local_heads
    blocks = length_total // BLOCK
    block_layout = (blocks, BLOCK, local_heads, head_width)
    reader = jax.nn.silu(query_matrix).reshape(block_layout)
    key_gate_value = jax.nn.sigmoid(-lower_bound_logits) * jax.nn.sigmoid(-forget_gate_logit)
    decay_logarithm = (
        jnp.log1p(-key_gate_value).reshape(length_total, local_heads, head_width)
        + decay_spike[0][:, :, None]
    ).reshape(block_layout)
    key_rows = key_gate_value.reshape(block_layout)
    value_rows = value_projected.reshape(block_layout)
    inner_log = jnp.cumsum(decay_logarithm, axis=1)
    read_scaled = reader * jnp.exp(inner_log)
    key_scaled = key_rows * jnp.exp(-inner_log)
    causal = (jnp.arange(BLOCK)[:, None] >= jnp.arange(BLOCK)[None, :]).astype(jnp.float32)
    scores = jnp.einsum("nthd,nshd->nhts", read_scaled, key_scaled, precision=HIGHEST) * causal
    within = jnp.einsum("nhts,nshe->nthe", scores, value_rows, precision=HIGHEST)
    closing = inner_log[:, -1]
    key_tail = key_rows * jnp.exp(closing[:, None] - inner_log)
    deltas = jnp.einsum("nshd,nshe->nhde", key_tail, value_rows, precision=HIGHEST)
    block_decay = jnp.exp(closing)

    def advance(carried, input_batch):
        decay_now, delta_now = input_batch
        return (decay_now[..., None] * carried + delta_now, carried)

    initial = jnp.zeros((local_heads, head_width, head_width), jnp.float32)
    device_state, entry_states = lax.scan(advance, initial, (block_decay, deltas))
    device_decay = jnp.exp(jnp.sum(closing, axis=0))
    scanned = entering(
        (device_decay, device_state),
        "sp",
        join_state,
        (jnp.ones_like(device_decay), jnp.zeros_like(device_state)),
    )
    prior_state = scanned[1]
    before = jnp.cumsum(closing, axis=0) - closing
    start_states = entry_states + jnp.exp(before)[..., None] * prior_state[None]
    read_out = within + jnp.einsum("nthd,nhde->nthe", read_scaled, start_states, precision=HIGHEST)
    read_out = read_out.reshape(length_total, local_heads, head_width)
    recurrent_output = (
        rms_scale(read_out, 1.0).reshape(length_total, rec_width) * head_norm_gain
    ).astype(jnp.bfloat16)
    mixed_rows = jnp.concatenate([pool_out, recurrent_output], axis=1)
    summed = lax.psum_scatter(
        jnp.dot(mixed_rows, out_full, preferred_element_type=jnp.float32).astype(jnp.bfloat16),
        "tp",
        scatter_dimension=0,
        tiled=True,
    )
    return summed[None]


F32 = jnp.float32
BF16 = jnp.bfloat16
NT = (((1,), (1,)), ((), ()))
TN = (((0,), (0,)), ((), ()))


def layer_kernel(
    n_sp, n_fs, n_tp,
    tok, gain, w_pool, w_query, w_forget, w_value, maps, scale, low, spike, hgain, w_po, w_ro,
    out,
    wbuf, tbuf, nbuf, sbuf, proj, pool_g, rec_g, part, dbuf, summed, obuf,
    wz_s, wz_r, wf_s, wf_r, tz_s, tz_r, td_s, td_r, ss_s, ss_r, pg_s, pg_r, rg_s, rg_r, d_s, d_r, o_s, o_r,
):
    s = lax.axis_index("sp")
    f = lax.axis_index("fs")
    t = lax.axis_index("tp")
    rows = tok.shape[0]
    depth = w_pool.shape[0]
    width = w_pool.shape[1] // n_sp
    piece = depth // n_fs
    length = n_sp * n_tp * rows
    weights = (w_pool, w_query, w_forget, w_value)

    def at(ds=0, df=0):
        return {"sp": lax.rem(s + ds, n_sp), "fs": lax.rem(f + df, n_fs), "tp": t}

    other = {"sp": s, "fs": f, "tp": 1 - t}

    def remote(src, dst, ssem, rsem, dev):
        return pltpu.make_async_remote_copy(
            src_ref=src, dst_ref=dst, send_sem=ssem, recv_sem=rsem,
            device_id=dev, device_id_type=pl.DeviceIdType.MESH,
        )

    barrier = pltpu.get_barrier_semaphore()
    partners = [at(ds=d) for d in range(1, n_sp)] + [at(df=e) for e in range(1, n_fs)] + [other]
    for dev in partners:
        pl.semaphore_signal(barrier, inc=1, device_id=dev, device_id_type=pl.DeviceIdType.MESH)
    pl.semaphore_wait(barrier, len(partners))

    def weight_copy(d, m):
        dest = lax.rem(s + d, n_sp)
        src = weights[m].at[pl.ds(pl.multiple_of(f * piece, piece), piece), pl.ds(pl.multiple_of(dest * width, width), width)]
        dst = wbuf.at[pl.ds(pl.multiple_of(s * depth + f * piece, piece), piece), pl.ds(m * width, width)]
        return remote(src, dst, wz_s.at[d - 1, m], wz_r.at[d - 1, m], at(ds=d))

    def weight_pass(d, e):
        origin = lax.rem(s - d + n_sp, n_sp)
        view = wbuf.at[pl.ds(pl.multiple_of(origin * depth + f * piece, piece), piece), :]
        return remote(view, view, wf_s.at[d - 1, e - 1], wf_r.at[d - 1, e - 1], at(df=e))

    def weight_received(d, e):
        origin = lax.rem(s - d + n_sp, n_sp)
        giver = lax.rem(f - e + n_fs, n_fs)
        view = wbuf.at[pl.ds(pl.multiple_of(origin * depth + giver * piece, piece), piece), :]
        return remote(view, view, wf_s.at[d - 1, e - 1], wf_r.at[d - 1, e - 1], at(df=e))

    def weight_arrival(d, m):
        origin = lax.rem(s - d + n_sp, n_sp)
        dst = wbuf.at[pl.ds(pl.multiple_of(origin * depth + f * piece, piece), piece), pl.ds(m * width, width)]
        return remote(dst, dst, wz_s.at[d - 1, m], wz_r.at[d - 1, m], at(ds=d))

    def spike_copy(d):
        dest = lax.rem(s + d, n_sp)
        return remote(spike.at[dest], sbuf.at[s], ss_s.at[d - 1], ss_r.at[d - 1], at(ds=d))

    def line(own, slots, send_sems, recv_sems):
        def sending(way, k):
            step = 1 - 2 * way
            origin = s - step * k
            dst = slots(origin)
            src = own if k == 0 else dst
            return remote(src, dst, send_sems.at[way, k], recv_sems.at[way, k], at(ds=step + n_sp))

        def arriving(way, k):
            step = 1 - 2 * way
            dst = slots(s - step * (k + 1))
            return remote(dst, dst, send_sems.at[way, k], recv_sems.at[way, k], at(ds=step + n_sp))

        def can_send(way, k):
            if way == 0:
                return jnp.logical_and(s - k >= 0, s + 1 < n_sp)
            return jnp.logical_and(s + k < n_sp, s - 1 >= 0)

        def will_arrive(way, k):
            return s - (k + 1) >= 0 if way == 0 else s + (k + 1) < n_sp

        return sending, arriving, can_send, will_arrive

    def hop_start(parts, k):
        sending, _, can_send, _ = parts
        for way in (0, 1):
            @pl.when(can_send(way, k))
            def _(way=way):
                sending(way, k).start()

    def hop_finish(parts):
        sending, _, can_send, _ = parts
        for k in range(n_sp - 1):
            for way in (0, 1):
                @pl.when(can_send(way, k))
                def _(way=way, k=k):
                    sending(way, k).wait_send()

    for d in (1, 3, 2) if n_sp == 4 else range(1, n_sp):
        for m in range(4):
            weight_copy(d, m).start()
    tokens_line = line(tok, lambda o: tbuf.at[o, t], tz_s, tz_r)
    hop_start(tokens_line, 0)
    own_pass = remote(tok, tbuf.at[s, t], td_s.at[s], td_r.at[s], other)
    own_pass.start()
    for d in range(1, n_sp):
        spike_copy(d).start()

    def core_pass(origin):
        view = tbuf.at[origin, t]
        return remote(view, view, td_s.at[origin], td_r.at[origin], other)

    def core_arrival(origin):
        view = tbuf.at[origin, 1 - t]
        return remote(view, view, td_s.at[origin], td_r.at[origin], other)

    gain_row = gain[...]

    def normalise(values, origin, core):
        x = values.astype(F32)
        y = x * lax.rsqrt(jnp.mean(x * x, axis=-1, keepdims=True) + EPSILON) * gain_row
        nbuf[origin, core] = y.astype(BF16)

    for m in range(4):
        wbuf[pl.ds(pl.multiple_of(s * depth, depth), depth), m * width:(m + 1) * width] = weights[m][
            :, pl.ds(pl.multiple_of(s * width, width), width)
        ]
    sbuf[s] = spike[s]
    normalise(tok[...], s, t)

    order = (1, 3, 2) if n_sp == 4 else tuple(range(1, n_sp))
    for d in order:
        for m in range(4):
            weight_arrival(d, m).wait_recv()
        for e in range(1, n_fs):
            weight_pass(d, e).start()
    def token_hop(k):
        for way in (0, 1):
            @pl.when(tokens_line[3](way, k))
            def _(way=way):
                origin = s - (1 - 2 * way) * (k + 1)
                tokens_line[1](way, k).wait_recv()
                if k + 1 < n_sp - 1:
                    @pl.when(tokens_line[2](way, k + 1))
                    def _():
                        tokens_line[0](way, k + 1).start()
                core_pass(origin).start()
        for way in (0, 1):
            @pl.when(tokens_line[3](way, k))
            def _(way=way):
                origin = s - (1 - 2 * way) * (k + 1)
                normalise(tbuf[origin, t], origin, t)

    def finish(origin):
        core_arrival(origin).wait_recv()
        normalise(tbuf[origin, 1 - t], origin, 1 - t)
        x = nbuf[origin].reshape(n_tp * rows, nbuf.shape[3])
        proj[origin] = jnp.dot(x, wbuf[...], preferred_element_type=F32).astype(BF16)

    for k in range(n_sp - 2):
        token_hop(k)
    for d in order:
        for e in range(1, n_fs):
            weight_received(d, e).wait_recv()
    for d in range(1, n_sp):
        dst = sbuf.at[lax.rem(s - d + n_sp, n_sp)]
        remote(dst, dst, ss_s.at[d - 1], ss_r.at[d - 1], at(ds=d)).wait_recv()

    near_low = jnp.maximum(s - (n_sp - 2), 0)
    near_high = jnp.minimum(s + (n_sp - 2), n_sp - 1)

    @pl.loop(0, n_sp)
    def _(origin):
        @pl.when(jnp.logical_and(origin >= near_low, origin <= near_high))
        def _():
            finish(origin)

    if n_sp > 1:
        token_hop(n_sp - 2)
    for way in (0, 1):
        @pl.when(tokens_line[3](way, n_sp - 2))
        def _(way=way):
            finish(s - (1 - 2 * way) * (n_sp - 1))

    projected = proj[...].reshape(length, 4 * width)
    x = projected[:, :width].astype(F32)
    group_size = maps.shape[1]
    groups = maps.shape[0]
    share = group_size // width
    group = t * groups + s // share
    position = lax.broadcasted_iota(jnp.int32, (length, width), 0)
    total = x
    window_sum = x
    window = jnp.int32(2)
    for g in range(n_tp * groups):
        reach = 2 ** g
        total = total + jnp.concatenate([jnp.zeros((reach, width), F32), total[: length - reach]], axis=0)
        window_sum = total if g == 0 else jnp.where(group == g, total, window_sum)
    for g in range(1, n_tp * groups):
        window = jnp.where(group == g, 2 ** (g + 1), window)
    counts = jnp.minimum(position + 1, window).astype(F32)
    pool_g[s] = (window_sum / counts - x).astype(BF16)
    pool_line = line(pool_g.at[s], lambda o: pool_g.at[o], pg_s, pg_r)
    hop_start(pool_line, 0)

    lows = low[s]
    tri_r = lax.broadcasted_iota(jnp.int32, (BLOCK, BLOCK), 0)
    tri_c = lax.broadcasted_iota(jnp.int32, (BLOCK, BLOCK), 1)
    causal = tri_r >= tri_c
    tri = causal.astype(F32)
    gate_low = jax.nn.sigmoid(-lows)
    state = jnp.zeros((width, width), F32)
    per_origin = length // n_sp
    columns = [jnp.transpose(sbuf[o])[:, :1] for o in range(n_sp)]
    for b in range(length // BLOCK):
        lo = b * BLOCK
        here = slice(lo, lo + BLOCK)
        q = projected[here, width:2 * width].astype(F32)
        logit = projected[here, 2 * width:3 * width].astype(F32)
        v = projected[here, 3 * width:]
        reader = q * jax.nn.sigmoid(q)
        key = gate_low * jax.nn.sigmoid(-logit)
        off = lo % per_origin
        logs = jnp.log1p(-key) + columns[lo // per_origin][off:off + BLOCK]
        inner = jnp.dot(tri, logs, preferred_element_type=F32, precision=HIGHEST)
        read_scaled = (reader * jnp.exp(inner)).astype(BF16)
        key_scaled = (key * jnp.exp(-inner)).astype(BF16)
        scores = lax.dot_general(read_scaled, key_scaled, NT, preferred_element_type=F32)
        scores = jnp.where(causal, scores, 0.0).astype(BF16)
        read = jnp.dot(scores, v, preferred_element_type=F32)
        read = read + lax.dot_general(read_scaled, state.astype(BF16), NT, preferred_element_type=F32)
        closing = inner[BLOCK - 1:]
        key_tail = (key * jnp.exp(closing - inner)).astype(BF16)
        state = jnp.exp(closing) * state + lax.dot_general(v, key_tail, TN, preferred_element_type=F32)
        rec = read * lax.rsqrt(jnp.mean(read * read, axis=-1, keepdims=True) + EPSILON) * hgain[s]
        rec_g[s, lo:lo + BLOCK] = rec.astype(BF16)
    strip = n_tp * rows
    strips = (0, 3, 1, 2) if n_sp == 4 else tuple(range(n_sp))

    def strip_line(p):
        here = pl.ds(p * strip, strip)
        return line(rec_g.at[s, here], lambda o: rec_g.at[o, here], rg_s.at[p], rg_r.at[p])

    rec_lines = [strip_line(p) for p in range(n_sp)]
    for p in strips:
        hop_start(rec_lines[p], 0)

    def relay(parts, k):
        for way in (0, 1):
            @pl.when(parts[3](way, k))
            def _(way=way):
                parts[1](way, k).wait_recv()
                if k + 1 < n_sp - 1:
                    @pl.when(parts[2](way, k + 1))
                    def _():
                        parts[0](way, k + 1).start()

    def across(p):
        return remote(part.at[1 - t, p], dbuf.at[p], d_s.at[p], d_r.at[p], other)

    def out_copy(p):
        return remote(summed.at[p], obuf.at[s], o_s.at[p], o_r.at[s], {"sp": p, "fs": f, "tp": t})

    def settle(p):
        across(p).wait_recv()
        summed[p] = (part[t, p].astype(F32) + dbuf[p].astype(F32)).astype(BF16)

        @pl.when(s != p)
        def _():
            out_copy(p).start()

        @pl.when(s == p)
        def _():
            obuf[p] = summed[p]

    for k in range(n_sp - 1):
        relay(pool_line, k)
        if k < n_sp - 2:
            for p in strips:
                relay(rec_lines[p], k)

    def project(p):
        here = slice(p * strip, (p + 1) * strip)
        mixed_row = []
        for g in range(groups):
            diff = jnp.concatenate([pool_g[g * share + c, here] for c in range(share)], axis=1)
            mapped = jnp.dot(diff, maps[g], preferred_element_type=F32)
            mixed_row.append((mapped * scale[:, g * group_size:(g + 1) * group_size]).astype(BF16))
        acc = jnp.dot(jnp.concatenate(mixed_row, axis=1), w_po[...], preferred_element_type=F32)
        recs = jnp.concatenate([rec_g[c, here] for c in range(n_sp)], axis=1)
        acc = acc + jnp.dot(recs, w_ro[...], preferred_element_type=F32)
        acc = acc.astype(BF16)
        for core in range(n_tp):
            part[core, p] = acc[core * rows:(core + 1) * rows]
        across(p).start()

    before = None
    for p in strips:
        relay(rec_lines[p], n_sp - 2)
        project(p)
        if before is not None:
            settle(before)
        before = p
    settle(before)

    for d in order:
        origin = lax.rem(s + d, n_sp)
        dst = obuf.at[origin]
        remote(dst, dst, o_s.at[origin], o_r.at[origin], at(ds=d)).wait_recv()
    cols = w_po.shape[1]
    for o in range(n_sp):
        out[:, o * cols:(o + 1) * cols] = obuf[o]

    for d in range(1, n_sp):
        for m in range(4):
            weight_copy(d, m).wait_send()
        for e in range(1, n_fs):
            weight_pass(d, e).wait_send()
        spike_copy(d).wait_send()
    hop_finish(tokens_line)
    hop_finish(pool_line)
    for p in range(n_sp):
        hop_finish(rec_lines[p])
        across(p).wait_send()

        @pl.when(s != p)
        def _(p=p):
            out_copy(p).wait_send()
    own_pass.wait_send()
    for k in range(n_sp - 1):
        for way in (0, 1):
            @pl.when(tokens_line[3](way, k))
            def _(way=way, k=k):
                core_pass(s - (1 - 2 * way) * (k + 1)).wait_send()


def head_body(sizes, *args):
    (tokens, gain, w_pool, w_query, w_forget, w_value, maps, scale, low, spike, hgain, w_po, w_ro) = args
    n_sp, n_fs, n_tp = sizes
    tok = tokens[0]
    rows, features = tok.shape
    width = w_pool.shape[1] // n_sp
    length = n_sp * n_tp * rows
    cols = w_po.shape[1]
    spikes = jnp.broadcast_to(spike[0].T[:, None, :], (spike.shape[2], 8, spike.shape[1]))
    dma = pltpu.SemaphoreType.DMA
    whole = pl.BlockSpec(memory_space=pltpu.VMEM)
    hop = (2, n_sp - 1)
    result = pl.pallas_call(
        functools.partial(layer_kernel, n_sp, n_fs, n_tp),
        out_shape=jax.ShapeDtypeStruct((rows, n_sp * cols), BF16),
        in_specs=[whole] * 13,
        out_specs=whole,
        scratch_shapes=[
            pltpu.VMEM((features, 4 * width), BF16),
            pltpu.VMEM((n_sp, n_tp, rows, features), BF16),
            pltpu.VMEM((n_sp, n_tp, rows, features), BF16),
            pltpu.VMEM((n_sp, 8, spike.shape[1]), F32),
            pltpu.VMEM((n_sp, n_tp * rows, 4 * width), BF16),
            pltpu.VMEM((n_sp, length, width), BF16),
            pltpu.VMEM((n_sp, length, width), BF16),
            pltpu.VMEM((n_tp, n_sp, rows, cols), BF16),
            pltpu.VMEM((n_sp, rows, cols), BF16),
            pltpu.VMEM((n_sp, rows, cols), BF16),
            pltpu.VMEM((n_sp, rows, cols), BF16),
            dma((n_sp - 1, 4)), dma((n_sp - 1, 4)),
            dma((n_sp - 1, n_fs - 1)), dma((n_sp - 1, n_fs - 1)),
            dma(hop), dma(hop),
            dma((n_sp,)), dma((n_sp,)),
            dma((n_sp - 1,)), dma((n_sp - 1,)),
            dma(hop), dma(hop),
            dma((n_sp,) + hop), dma((n_sp,) + hop),
            dma((n_sp,)), dma((n_sp,)),
            dma((n_sp,)), dma((n_sp,)),
        ],
        compiler_params=pltpu.CompilerParams(
            collective_id=0, has_side_effects=True, vmem_limit_bytes=56 * 1024 * 1024
        ),
        name="layer",
    )(
        tok, gain[None], w_pool, w_query, w_forget, w_value, maps, scale[None],
        low.reshape(n_sp, 1, width), spikes, hgain.reshape(n_sp, 1, width), w_po, w_ro,
    )
    return result[None]


def solution(mesh):
    placed = (
        P("fs", ("sp", "tp"), None),
        P(),
        P("sp", "tp"),
        P("sp", "tp"),
        P("sp", "tp"),
        P("sp", "tp"),
        P("tp", None, None),
        P("tp"),
        P("tp"),
        P("fs", "sp", "tp"),
        P("tp"),
        P("tp", "sp"),
        P("tp", "sp"),
    )
    sizes = (mesh.shape["sp"], mesh.shape["fs"], mesh.shape["tp"])

    def one(*args):
        maps, spike = args[6], args[9]
        width = args[2].shape[1] // sizes[0]
        fits = spike.shape[2] == sizes[0] and sizes[2] == 2 and width % 128 == 0
        fits = fits and args[3].shape[1] == args[2].shape[1] and maps.shape[1] % width == 0
        return head_body(sizes, *args) if fits else body(*args)

    return jax.shard_map(
        one, mesh=mesh, in_specs=placed, out_specs=P("fs", ("sp", "tp"), None), check_vma=False
    )
```

profile of v0, /device:TPU:0, one launch (start us, length us, event | category | flops | bytes accessed | tf_op | source)
XLA Modules:
  0.0 69.9 jit_solution(4072434945456612581)
XLA Ops:
  0.0 0.0 copy-start
  0.0 0.7 copy-done
  0.7 0.6 broadcast_in_dim.17.spike
  1.3 66.9 %layer.1 = bf16[64,2048]{1,0:T(8,128)(2,1)} custom-call(bf16[64,2048]{1,0:T(8,128)(2,1)} %bitcast.10, f32[1,2048]{1,0:T(1,128)} %bitcast.11, bf16[512,512]{1,0:T(8,128)(2,1)} %w_pool.1, bf16[512,512]{1,0:T(8,128)(2,1)} %w_query.1, bf16[512,512]{1,0:T(8,128)(2,1)} %w_forget.1, bf16[512,512]{1,0:T(8,128)(2,1)} %w_value.1, bf16[2,256,256]{2,1,0:T(8,128)(2,1)} %maps.1, ...), custom_call_target="tpu_custom_call" | custom-call | tf_op jit(solution)/shard_map/layer/pallas_call | solution.py:525
  68.2 1.7 %copy.15 = bf16[1,64,2048]{2,1,0:T(8,128)(2,1)} copy(bf16[1,64,2048]{2,1,0:T(8,128)(2,1)} %bitcast.9) | data formatting | bytes 524288
Async XLA Ops:
  0.0 0.7 copy-start
where the time goes:
time: 70.1 us; the launch traced here: 69.9 us
  Pallas kernels  66.9 us (95%)
  local copies, waits for them, and re-layouts  2.96 us (4%)
    pallas_call x1, Pallas kernels, head_body(): pl.pallas_call(functools.partial(layer_kernel, n_sp, n_fs, n_tp), out_sha...  66.9 us
    unnamed x3, local copies, waits for them, and re-layouts  2.35 us

commit v1 on v0

v1 whole, which is shorter than its diff:
```python
import functools

import jax
import jax.numpy as jnp
from jax import lax
from jax.experimental import pallas as pl
from jax.experimental.pallas import tpu as pltpu
from jax.sharding import PartitionSpec as P

BLOCK = 64


EPSILON = 1e-06
HIGHEST = lax.Precision.HIGHEST


def shifted(value, axis, steps):
    count = lax.axis_size(axis)
    first, last = (max(0, -steps), min(count, count - steps))
    return lax.ppermute(value, axis, [(source, source + steps) for source in range(first, last)])


def entering(shard, axis, join, neutral):
    place = lax.axis_index(axis)
    gathered = jax.tree.map(
        lambda a, kind: lax.all_gather(a.astype(kind), axis), shard, (jnp.bfloat16, jnp.bfloat16)
    )
    state = jax.tree.map(lambda a, e: jnp.zeros_like(a) + jnp.asarray(e, a.dtype), shard, neutral)

    def one(step, state):
        return join(
            state,
            jax.tree.map(
                lambda a, own: lax.dynamic_index_in_dim(a, step, 0, False).astype(own.dtype),
                gathered,
                shard,
            ),
        )

    return lax.fori_loop(0, place, one, state)


def rms_scale(values, gain):
    return values * lax.rsqrt(jnp.mean(values * values, axis=-1, keepdims=True) + EPSILON) * gain


def join_state(earlier, later):
    decay_one, state_one = earlier
    decay_two, state_two = later
    return (decay_one * decay_two, decay_two[..., None] * state_one + state_two)


def body(
    tokens,
    input_norm_gain,
    pooling_input_weight,
    query_weight,
    forget_weight,
    value_weight,
    pooling_group_maps,
    pooling_scale,
    lower_bound_logits,
    decay_spike,
    head_norm_gain,
    pooling_output_weight,
    recurrent_output_weight,
):
    gathered = lax.all_gather(tokens, "tp", axis=1, tiled=True)[0]
    length_total = gathered.shape[0]
    normed = rms_scale(gathered.astype(jnp.float32), input_norm_gain).astype(jnp.bfloat16)
    pool_width = pooling_input_weight.shape[1]
    rec_width = query_weight.shape[1]
    stacked = jnp.concatenate(
        [pooling_input_weight, query_weight, forget_weight, value_weight], axis=1
    )
    out_local = jnp.concatenate([pooling_output_weight, recurrent_output_weight], axis=0)
    groups_fs = lax.axis_size("fs")
    member = lax.axis_index("fs")
    slice_width = stacked.shape[1] // groups_fs
    own_slice = lax.dynamic_slice_in_dim(stacked, member * slice_width, slice_width, 1)
    column_part = lax.all_gather(own_slice, "sp", axis=0, tiled=True)
    full_input = lax.all_gather(column_part, "fs", axis=1, tiled=True)
    projected = jnp.dot(normed, full_input, preferred_element_type=jnp.float32)
    slice_height = out_local.shape[0] // groups_fs
    own_rows = lax.dynamic_slice_in_dim(out_local, member * slice_height, slice_height, 0)
    row_part = lax.all_gather(own_rows, "sp", axis=1, tiled=True)
    out_full = lax.all_gather(row_part, "fs", axis=0, tiled=True)
    rounded = lax.optimization_barrier(projected.astype(jnp.bfloat16))
    pool_input = rounded[:, :pool_width]
    query_matrix = rounded[:, pool_width : pool_width + rec_width].astype(jnp.float32)
    forget_gate_logit = rounded[:, pool_width + rec_width : pool_width + 2 * rec_width].astype(
        jnp.float32
    )
    value_projected = rounded[:, pool_width + 2 * rec_width :].astype(jnp.float32)
    groups_local = pooling_group_maps.shape[0]
    group_size = pooling_group_maps.shape[1]
    reach_rows = 2 ** (groups_local * lax.axis_size("tp"))
    previous = shifted(pool_input[length_total - reach_rows :], "sp", 1)
    extended = jnp.concatenate([previous, pool_input], axis=0).astype(jnp.float32)
    extended = extended.reshape(reach_rows + length_total, groups_local, group_size)
    group_ids = lax.axis_index("tp") * groups_local + jnp.arange(groups_local, dtype=jnp.int32)
    windows = jnp.left_shift(jnp.int32(2), group_ids)
    window_sum = jnp.zeros((length_total, groups_local, group_size), jnp.float32)
    for offset in range(reach_rows):
        inside = (offset < windows).astype(jnp.float32)
        window_sum = (
            window_sum
            + extended[reach_rows - offset : reach_rows - offset + length_total] * inside[:, None]
        )
    position_index = lax.axis_index("sp") * length_total + jnp.arange(length_total, dtype=jnp.int32)
    counts = jnp.minimum(position_index[:, None] + 1, windows[None, :]).astype(jnp.float32)
    pool_diff = (window_sum / counts[:, :, None] - extended[reach_rows:]).astype(jnp.bfloat16)
    pool_mapped = jnp.einsum(
        "tgc,gcd->tgd", pool_diff, pooling_group_maps, preferred_element_type=jnp.float32
    )
    pool_out = (pool_mapped.reshape(length_total, pool_width) * pooling_scale).astype(jnp.bfloat16)
    local_heads = decay_spike.shape[2]
    head_width = rec_width // local_heads
    blocks = length_total // BLOCK
    block_layout = (blocks, BLOCK, local_heads, head_width)
    reader = jax.nn.silu(query_matrix).reshape(block_layout)
    key_gate_value = jax.nn.sigmoid(-lower_bound_logits) * jax.nn.sigmoid(-forget_gate_logit)
    decay_logarithm = (
        jnp.log1p(-key_gate_value).reshape(length_total, local_heads, head_width)
        + decay_spike[0][:, :, None]
    ).reshape(block_layout)
    key_rows = key_gate_value.reshape(block_layout)
    value_rows = value_projected.reshape(block_layout)
    inner_log = jnp.cumsum(decay_logarithm, axis=1)
    read_scaled = reader * jnp.exp(inner_log)
    key_scaled = key_rows * jnp.exp(-inner_log)
    causal = (jnp.arange(BLOCK)[:, None] >= jnp.arange(BLOCK)[None, :]).astype(jnp.float32)
    scores = jnp.einsum("nthd,nshd->nhts", read_scaled, key_scaled, precision=HIGHEST) * causal
    within = jnp.einsum("nhts,nshe->nthe", scores, value_rows, precision=HIGHEST)
    closing = inner_log[:, -1]
    key_tail = key_rows * jnp.exp(closing[:, None] - inner_log)
    deltas = jnp.einsum("nshd,nshe->nhde", key_tail, value_rows, precision=HIGHEST)
    block_decay = jnp.exp(closing)

    def advance(carried, input_batch):
        decay_now, delta_now = input_batch
        return (decay_now[..., None] * carried + delta_now, carried)

    initial = jnp.zeros((local_heads, head_width, head_width), jnp.float32)
    device_state, entry_states = lax.scan(advance, initial, (block_decay, deltas))
    device_decay = jnp.exp(jnp.sum(closing, axis=0))
    scanned = entering(
        (device_decay, device_state),
        "sp",
        join_state,
        (jnp.ones_like(device_decay), jnp.zeros_like(device_state)),
    )
    prior_state = scanned[1]
    before = jnp.cumsum(closing, axis=0) - closing
    start_states = entry_states + jnp.exp(before)[..., None] * prior_state[None]
    read_out = within + jnp.einsum("nthd,nhde->nthe", read_scaled, start_states, precision=HIGHEST)
    read_out = read_out.reshape(length_total, local_heads, head_width)
    recurrent_output = (
        rms_scale(read_out, 1.0).reshape(length_total, rec_width) * head_norm_gain
    ).astype(jnp.bfloat16)
    mixed_rows = jnp.concatenate([pool_out, recurrent_output], axis=1)
    summed = lax.psum_scatter(
        jnp.dot(mixed_rows, out_full, preferred_element_type=jnp.float32).astype(jnp.bfloat16),
        "tp",
        scatter_dimension=0,
        tiled=True,
    )
    return summed[None]


F32 = jnp.float32
BF16 = jnp.bfloat16
NT = (((1,), (1,)), ((), ()))
TN = (((0,), (0,)), ((), ()))

CHUNKS = 4


def layer_kernel(
    n_fs, n_tp,
    tok, gain, w_pool, w_query, w_forget, w_value, maps, scale, low, spike, hgain, w_po, w_ro,
    out,
    tbuf, stage, wbuf, nbuf, sbuf, proj, pool_g, rec_g, wo, map_v, pacc, part, dbuf, summed, obuf,
    ld, w_s, w_r, wt_s, wt_r, sp_s, sp_r, tz_s, tz_r, tq_s, td_s, td_r,
    wo_s, wo_r, ot_s, ot_r, pg_s, pg_r, pq_s, rg_s, rg_r, rq_s, d_s, d_r, o_s, o_r,
):
    s = lax.axis_index("sp")
    f = lax.axis_index("fs")
    t = lax.axis_index("tp")
    n_sp = 4
    rows = tok.shape[0]
    depth = w_pool.shape[0]
    width = w_pool.shape[1] // n_sp
    cols = w_po.shape[1]
    piece = depth // n_fs
    half = piece // 2
    strip = n_tp * rows
    length = n_sp * strip
    weights = (w_pool, w_query, w_forget, w_value)

    side = s // 2
    end, mid, omid, oend = 3 * side, 1 + side, 2 - side, 3 - 3 * side
    mate = end + mid - s
    is_end, is_mid = s == end, s == mid
    peers = (mate, omid, oend)

    def z(o):
        return {"sp": o, "fs": f, "tp": t}

    at_x = {"sp": s, "fs": f + 1 - 2 * lax.rem(f, 2), "tp": t}
    at_y = {"sp": s, "fs": f + 2 - 4 * (f // 2), "tp": t}
    other = {"sp": s, "fs": f, "tp": 1 - t}
    f_x, f_y, f_d = at_x["fs"], at_y["fs"], 3 - f

    def ds(start, size):
        return pl.ds(pl.multiple_of(start, size), size)

    def remote(src, dst, ssem, rsem, dev):
        return pltpu.make_async_remote_copy(
            src_ref=src, dst_ref=dst, send_sem=ssem, recv_sem=rsem,
            device_id=dev, device_id_type=pl.DeviceIdType.MESH,
        )

    drains = []

    def send(copy, cond=None, drain_cond=None):
        if cond is None:
            copy.start()
        else:
            pl.when(cond)(copy.start)
        drains.append((drain_cond if cond is None else cond, copy))

    def load(src, dst, i):
        copy = pltpu.make_async_copy(src, dst, ld.at[i])
        copy.start()
        return copy

    tok_load = load(tok, tbuf, 0)
    stage_loads = [
        [
            load(
                weights[m].at[ds(f * piece, piece), ds(dest * width, width)],
                stage.at[j, :, pl.ds(m * width, width)],
                1 + 4 * j + m,
            )
            for m in range(4)
        ]
        for j, dest in enumerate(peers)
    ]
    own_loads = [
        load(
            weights[m].at[:, ds(s * width, width)],
            wbuf.at[ds(s * depth, depth), pl.ds(m * width, width)],
            13 + m,
        )
        for m in range(4)
    ]
    late_loads = [
        load(maps, map_v, 17),
        load(w_po, wo.at[0, :, ds(lax.rem(s, 2) * cols, cols)], 18),
        load(w_ro, wo.at[1, :, ds(lax.rem(s, 2) * cols, cols)], 19),
    ]

    barrier = pltpu.get_barrier_semaphore()
    partners = [z(o) for o in peers] + [at_x, at_y, other]
    for dev in partners:
        pl.semaphore_signal(barrier, inc=1, device_id=dev, device_id_type=pl.DeviceIdType.MESH)
    pl.semaphore_wait(barrier, len(partners))

    def w_view(o, giver, h=None):
        if h is None:
            return wbuf.at[ds(o * depth + giver * piece, piece), :]
        return wbuf.at[ds(o * depth + giver * piece + h * half, half), :]

    def wo_view(k, giver, h=None):
        place = ds(lax.rem(end, 2) * cols, cols)
        if h is None:
            return wo.at[k, ds(giver * piece, piece), place]
        return wo.at[k, ds(giver * piece + h * half, half), place]

    def tree(view, ssem, rsem):
        def first(i, o):
            mine = view(o, f)
            send(remote(mine, mine, ssem.at[0, i], rsem.at[0, i], at_x))
            send(remote(mine, mine, ssem.at[1, i], rsem.at[1, i], at_y))

        def second(i, o):
            got = view(o, f_x)
            remote(got, got, ssem.at[0, i], rsem.at[0, i], at_x).wait_recv()
            on = view(o, f_x, 0)
            send(remote(on, on, ssem.at[2, i], rsem.at[2, i], at_y))
            got = view(o, f_y)
            remote(got, got, ssem.at[1, i], rsem.at[1, i], at_y).wait_recv()
            on = view(o, f_y, 1)
            send(remote(on, on, ssem.at[3, i], rsem.at[3, i], at_x))

        def last(i, o):
            got = view(o, f_d, 0)
            remote(got, got, ssem.at[2, i], rsem.at[2, i], at_y).wait_recv()
            got = view(o, f_d, 1)
            remote(got, got, ssem.at[3, i], rsem.at[3, i], at_x).wait_recv()

        return first, second, last

    for j, dest in enumerate(peers):
        for copy in stage_loads[j]:
            copy.wait()
        send(remote(stage.at[j], w_view(s, f), w_s.at[j], w_r.at[s], z(dest)))
    for j, dest in enumerate(peers):
        send(remote(spike, sbuf.at[s], sp_s.at[j], sp_r.at[s], z(dest)))

    chunk = rows // CHUNKS

    def tok_view(o, core, c):
        return nbuf.at[o, core, pl.ds(c * chunk, chunk), :]

    def core_pass(o, c):
        view = tok_view(o, t, c)
        send(remote(view, view, td_s.at[o, c], td_r.at[o, c], other))

    def core_arrival(o):
        for c in range(CHUNKS):
            view = tok_view(o, 1 - t, c)
            remote(view, view, td_s.at[o, c], td_r.at[o, c], other).wait_recv()

    def tok_arrival(o, c):
        view = tok_view(o, t, c)
        remote(view, view, tz_s.at[0, c], tz_r.at[o, c], z(o)).wait_recv()

    tok_load.wait()
    gain_row = gain[...]
    x = tbuf[...].astype(F32)
    y = x * lax.rsqrt(jnp.mean(x * x, axis=-1, keepdims=True) + EPSILON) * gain_row
    nbuf[s, t] = y.astype(BF16)
    for j, dest in enumerate((omid, mate)):
        for c in range(CHUNKS):
            view = tok_view(s, t, c)
            send(remote(view, view, tz_s.at[j, c], tz_r.at[s, c], z(dest)))
    for c in range(CHUNKS):
        core_pass(s, c)
    for k, w_out in enumerate((w_po, w_ro)):
        dst = wo.at[k, ds(f * piece, piece), ds(lax.rem(s, 2) * cols, cols)]
        send(remote(w_out.at[ds(f * piece, piece), :], dst, wo_s.at[k], wo_r.at[k], z(mid)), is_end)
    sbuf[s] = spike[...]

    first, second, last = tree(w_view, wt_s, wt_r)

    def w_arrival(j):
        view = w_view(peers[j], f)
        remote(view, view, w_s.at[j], w_r.at[peers[j]], z(peers[j])).wait_recv()

    w_arrival(0)
    first(0, peers[0])
    w_arrival(1)
    first(1, peers[1])
    second(0, peers[0])
    w_arrival(2)
    first(2, peers[2])
    second(1, peers[1])
    second(2, peers[2])

    far = (omid, oend)
    relays = [
        [remote(tok_view(o, t, c), tok_view(o, t, c), tq_s.at[k, c], tz_r.at[o, c], z(end)) for c in range(CHUNKS)]
        for k, o in enumerate(far)
    ]
    passes = [
        [remote(tok_view(o, t, c), tok_view(o, t, c), td_s.at[o, c], td_r.at[o, c], other) for c in range(CHUNKS)]
        for o in far
    ]

    @pl.when(is_mid)
    def _():
        for c in range(CHUNKS):
            for k, o in enumerate(far):
                tok_arrival(o, c)
                relays[k][c].start()
                passes[k][c].start()

    for c in range(CHUNKS):
        tok_arrival(mate, c)
        core_pass(mate, c)
    for j in range(3):
        last(j, peers[j])
    for copy in own_loads:
        copy.wait()
    core_arrival(s)
    core_arrival(mate)

    def project(base):
        x = nbuf[pl.ds(base, 2)].reshape(2 * strip, nbuf.shape[3])
        y = jnp.dot(x, wbuf[...], preferred_element_type=F32)
        proj[pl.ds(base, 2)] = y.astype(BF16).reshape(2, strip, 4 * width)

    project(2 * side)

    @pl.when(is_end)
    def _():
        for c in range(CHUNKS):
            for k, o in enumerate(far):
                tok_arrival(o, c)
                passes[k][c].start()

    core_arrival(omid)
    core_arrival(oend)
    project(2 - 2 * side)
    for k in range(2):
        for c in range(CHUNKS):
            drains.append((is_mid, relays[k][c]))
            drains.append((None, passes[k][c]))

    target = 1 + lax.rem(s, 2)
    projected = proj[...].reshape(length, 4 * width)
    x = projected[:, :width].astype(F32)
    group_size = maps.shape[1]
    groups = maps.shape[0]
    share = group_size // width
    group = t * groups + s // share
    position = lax.broadcasted_iota(jnp.int32, (length, width), 0)
    total = x
    window_sum = x
    window = jnp.int32(2)
    for g in range(n_tp * groups):
        reach = 2 ** g
        total = total + jnp.concatenate([jnp.zeros((reach, width), F32), total[: length - reach]], axis=0)
        window_sum = total if g == 0 else jnp.where(group == g, total, window_sum)
    for g in range(1, n_tp * groups):
        window = jnp.where(group == g, 2 ** (g + 1), window)
    counts = jnp.minimum(position + 1, window).astype(F32)
    pool_g[s] = (window_sum / counts - x).astype(BF16)
    send(remote(pool_g.at[s], pool_g.at[s], pg_s.at[0], pg_r.at[s], z(target)))

    wo_first, wo_second, wo_last = tree(wo_view, ot_s, ot_r)
    tree_from = len(drains)

    @pl.when(is_mid)
    def _():
        for copy in late_loads[1:]:
            copy.wait()
        for k in range(2):
            view = wo_view(k, f)
            remote(view, view, wo_s.at[k], wo_r.at[k], z(end)).wait_recv()
            mine = wo_view(k, f)
            remote(mine, mine, ot_s.at[0, k], ot_r.at[0, k], at_x).start()
            remote(mine, mine, ot_s.at[1, k], ot_r.at[1, k], at_y).start()

    for d in range(1, n_sp):
        o = lax.rem(s + d, n_sp)
        remote(spike, sbuf.at[o], sp_s.at[d - 1], sp_r.at[o], z(o)).wait_recv()
    lows = low[s]
    tri_r = lax.broadcasted_iota(jnp.int32, (BLOCK, BLOCK), 0)
    tri_c = lax.broadcasted_iota(jnp.int32, (BLOCK, BLOCK), 1)
    causal = tri_r >= tri_c
    tri = causal.astype(F32)
    gate_low = jax.nn.sigmoid(-lows)
    state = jnp.zeros((width, width), F32)
    columns = [jnp.transpose(jnp.broadcast_to(sbuf[o, pl.ds(s, 1)], (8, strip)))[:, :1] for o in range(n_sp)]
    for b in range(length // BLOCK):
        lo = b * BLOCK
        here = slice(lo, lo + BLOCK)
        q = projected[here, width:2 * width].astype(F32)
        logit = projected[here, 2 * width:3 * width].astype(F32)
        v = projected[here, 3 * width:]
        reader = q * jax.nn.sigmoid(q)
        key = gate_low * jax.nn.sigmoid(-logit)
        off = lo % strip
        logs = jnp.log1p(-key) + columns[lo // strip][off:off + BLOCK]
        inner = jnp.dot(tri, logs, preferred_element_type=F32, precision=HIGHEST)
        read_scaled = (reader * jnp.exp(inner)).astype(BF16)
        key_scaled = (key * jnp.exp(-inner)).astype(BF16)
        scores = lax.dot_general(read_scaled, key_scaled, NT, preferred_element_type=F32)
        scores = jnp.where(causal, scores, 0.0).astype(BF16)
        read = jnp.dot(scores, v, preferred_element_type=F32)
        read = read + lax.dot_general(read_scaled, state.astype(BF16), NT, preferred_element_type=F32)
        closing = inner[BLOCK - 1:]
        key_tail = (key * jnp.exp(closing - inner)).astype(BF16)
        state = jnp.exp(closing) * state + lax.dot_general(v, key_tail, TN, preferred_element_type=F32)
        rec = read * lax.rsqrt(jnp.mean(read * read, axis=-1, keepdims=True) + EPSILON) * hgain[s]
        rec_g[s, lo:lo + BLOCK] = rec.astype(BF16)

    def rec_view(o, p):
        return rec_g.at[o, ds(p * strip, strip), :]

    order = (oend, end, omid, mid)
    for p in order:
        view = rec_view(s, p)
        send(remote(view, view, rg_s.at[p], rg_r.at[s, p], z(target)))

    def pool_arrival(o):
        view = pool_g.at[o]
        remote(view, view, pg_s.at[0], pg_r.at[o], z(o)).wait_recv()

    def rec_arrival(o, p):
        view = rec_view(o, p)
        remote(view, view, rg_s.at[p], rg_r.at[o, p], z(o)).wait_recv()

    pool_relay = remote(pool_g.at[end], pool_g.at[end], pq_s.at[0], pg_r.at[end], z(omid))
    rec_relays = [
        remote(rec_view(end, p), rec_view(end, p), rq_s.at[p], rg_r.at[end, p], z(omid)) for p in order
    ]
    blocks = (oend, omid, end, mid)

    def across(i):
        return remote(part.at[i, 1 - t], dbuf.at[i], d_s.at[i], d_r.at[i], other)

    def deliver(i):
        return remote(summed.at[i], obuf.at[side], o_s.at[i], o_r.at[side], z(blocks[i]))

    @pl.when(is_mid)
    def _():
        pool_arrival(end)
        pool_relay.start()
        for k in range(2):
            mark = len(drains)
            wo_second(k, k)
            del drains[mark:]
        for i, p in enumerate(order):
            rec_arrival(end, p)
            rec_relays[i].start()
        late_loads[0].wait()
        for k in range(2):
            wo_last(k, k)
        pool_arrival(omid)
        pool_arrival(oend)
        mixed = []
        for g in range(groups):
            diff = jnp.concatenate([pool_g[g * share + c] for c in range(share)], axis=1)
            mapped = jnp.dot(diff, map_v[g], preferred_element_type=F32)
            mixed.append((mapped * scale[:, g * group_size:(g + 1) * group_size]).astype(BF16))
        pacc[...] = jnp.dot(jnp.concatenate(mixed, axis=1), wo[0], preferred_element_type=F32)

        def settle(i):
            across(i).wait_recv()
            both = (part[i, t].astype(F32) + dbuf[i].astype(F32)).astype(BF16)
            if i < 3:
                summed[i] = both
                deliver(i).start()
            else:
                obuf[side] = both

        for i, p in enumerate(blocks):
            rec_arrival(omid, p)
            rec_arrival(oend, p)
            recs = jnp.concatenate([rec_g[c, ds(p * strip, strip), :] for c in range(n_sp)], axis=1)
            acc = pacc[ds(p * strip, strip), :] + jnp.dot(recs, wo[1], preferred_element_type=F32)
            acc = acc.astype(BF16)
            for core in range(n_tp):
                part[i, core] = acc[core * rows:(core + 1) * rows]
            across(i).start()
            if i > 0:
                settle(i - 1)
        settle(3)

    @pl.when(is_end)
    def _():
        for copy in late_loads:
            copy.wait()
        view = obuf.at[side]
        remote(view, view, o_s.at[0], o_r.at[side], z(mid)).wait_recv()

    view = obuf.at[1 - side]
    remote(view, view, o_s.at[0], o_r.at[1 - side], z(omid)).wait_recv()
    for h in range(2):
        out[:, 2 * h * cols:2 * (h + 1) * cols] = obuf[h]

    for cond, copy in drains:
        if cond is None:
            copy.wait_send()
        else:
            pl.when(cond)(copy.wait_send)

    @pl.when(is_mid)
    def _():
        pool_relay.wait_send()
        for copy in rec_relays:
            copy.wait_send()
        for i in range(4):
            across(i).wait_send()
        for i in range(3):
            deliver(i).wait_send()
        for k in range(2):
            mine = wo_view(k, f)
            remote(mine, mine, ot_s.at[0, k], ot_r.at[0, k], at_x).wait_send()
            remote(mine, mine, ot_s.at[1, k], ot_r.at[1, k], at_y).wait_send()
            on = wo_view(k, f_x, 0)
            remote(on, on, ot_s.at[2, k], ot_r.at[2, k], at_y).wait_send()
            on = wo_view(k, f_y, 1)
            remote(on, on, ot_s.at[3, k], ot_r.at[3, k], at_x).wait_send()


def head_body(sizes, *args):
    (tokens, gain, w_pool, w_query, w_forget, w_value, maps, scale, low, spike, hgain, w_po, w_ro) = args
    n_sp, n_fs, n_tp = sizes
    tok = tokens[0]
    rows, features = tok.shape
    depth = w_pool.shape[0]
    width = w_pool.shape[1] // n_sp
    length = n_sp * n_tp * rows
    cols = w_po.shape[1]
    dma = pltpu.SemaphoreType.DMA
    whole = pl.BlockSpec(memory_space=pltpu.VMEM)
    here = pl.BlockSpec(memory_space=pl.ANY)
    result = pl.pallas_call(
        functools.partial(layer_kernel, n_fs, n_tp),
        out_shape=jax.ShapeDtypeStruct((rows, n_sp * cols), BF16),
        in_specs=[here, whole, here, here, here, here, here, whole, whole, whole, whole, here, here],
        out_specs=whole,
        scratch_shapes=[
            pltpu.VMEM((rows, features), BF16),
            pltpu.VMEM((3, depth // n_fs, 4 * width), BF16),
            pltpu.VMEM((features, 4 * width), BF16),
            pltpu.VMEM((n_sp, n_tp, rows, features), BF16),
            pltpu.VMEM((n_sp,) + (spike.shape[2], spike.shape[1]), F32),
            pltpu.VMEM((n_sp, n_tp * rows, 4 * width), BF16),
            pltpu.VMEM((n_sp, length, width), BF16),
            pltpu.VMEM((n_sp, length, width), BF16),
            pltpu.VMEM((2, w_po.shape[0], 2 * cols), BF16),
            pltpu.VMEM(maps.shape, BF16),
            pltpu.VMEM((length, 2 * cols), F32),
            pltpu.VMEM((n_sp, n_tp, rows, 2 * cols), BF16),
            pltpu.VMEM((n_sp, rows, 2 * cols), BF16),
            pltpu.VMEM((n_sp, rows, 2 * cols), BF16),
            pltpu.VMEM((2, rows, 2 * cols), BF16),
            dma((20,)),
            dma((3,)), dma((n_sp,)),
            dma((4, 3)), dma((4, 3)),
            dma((3,)), dma((n_sp,)),
            dma((2, CHUNKS)), dma((n_sp, CHUNKS)), dma((2, CHUNKS)),
            dma((n_sp, CHUNKS)), dma((n_sp, CHUNKS)),
            dma((2,)), dma((2,)),
            dma((4, 2)), dma((4, 2)),
            dma((1,)), dma((n_sp,)), dma((1,)),
            dma((n_sp,)), dma((n_sp, n_sp)), dma((n_sp,)),
            dma((n_sp,)), dma((n_sp,)),
            dma((n_sp,)), dma((2,)),
        ],
        compiler_params=pltpu.CompilerParams(
            collective_id=0, has_side_effects=True, vmem_limit_bytes=56 * 1024 * 1024
        ),
        name="layer",
    )(
        tok, gain[None], w_pool, w_query, w_forget, w_value, maps, scale[None],
        low.reshape(n_sp, 1, width), spike[0].T, hgain.reshape(n_sp, 1, width), w_po, w_ro,
    )
    return result[None]


def solution(mesh):
    placed = (
        P("fs", ("sp", "tp"), None),
        P(),
        P("sp", "tp"),
        P("sp", "tp"),
        P("sp", "tp"),
        P("sp", "tp"),
        P("tp", None, None),
        P("tp"),
        P("tp"),
        P("fs", "sp", "tp"),
        P("tp"),
        P("tp", "sp"),
        P("tp", "sp"),
    )
    sizes = (mesh.shape["sp"], mesh.shape["fs"], mesh.shape["tp"])

    def one(*args):
        maps, spike = args[6], args[9]
        width = args[2].shape[1] // sizes[0]
        fits = spike.shape[2] == sizes[0] and sizes == (4, 4, 2) and width % 128 == 0
        fits = fits and args[3].shape[1] == args[2].shape[1] and maps.shape[1] % width == 0
        return head_body(sizes, *args) if fits else body(*args)

    return jax.shard_map(
        one, mesh=mesh, in_specs=placed, out_specs=P("fs", ("sp", "tp"), None), check_vma=False
    )
```

time: 70.1 us -> 63.8 us (0.910)
  Pallas kernels: 66.9 us -> 62 us
  local copies, waits for them, and re-layouts: 2.96 us -> 1.67 us
    pallas_call x1, Pallas kernels: 66.9 us -> 62 us  [head_body(): pl.pallas_call(functools.partial(layer_kernel, n_fs, n_tp), out_shape=jax...]
    unnamed x3 -> x1, local copies, waits for them, and re-layouts: 2.35 us -> 1.67 us
where the time goes in v1:
time: 63.8 us; the launch traced here: 63.6 us
  Pallas kernels  62 us (97%)
  local copies, waits for them, and re-layouts  1.67 us (3%)
    pallas_call x1, Pallas kernels, head_body(): pl.pallas_call(functools.partial(layer_kernel, n_fs, n_tp), out_shape=jax...  62 us
    unnamed x1, local copies, waits for them, and re-layouts  1.67 us

profile of v1, /device:TPU:0, one launch (start us, length us, event | category | flops | bytes accessed | tf_op | source)
XLA Modules:
  0.0 63.6 jit_solution(4872620076218034303)
XLA Ops:
  0.0 62.0 %layer.1 = bf16[64,2048]{1,0:T(8,128)(2,1)} custom-call(bf16[64,2048]{1,0:T(8,128)(2,1)} %bitcast.10, f32[1,2048]{1,0:T(1,128)} %bitcast.11, bf16[512,512]{1,0:T(8,128)(2,1)} %w_pool.1, bf16[512,512]{1,0:T(8,128)(2,1)} %w_query.1, bf16[512,512]{1,0:T(8,128)(2,1)} %w_forget.1, bf16[512,512]{1,0:T(8,128)(2,1)} %w_value.1, bf16[2,256,256]{2,1,0:T(8,128)(2,1)} %maps.1, ...), custom_call_target="tpu_custom_call" | custom-call | tf_op jit(solution)/shard_map/layer/pallas_call | solution.py:603
  62.0 1.7 %copy.15 = bf16[1,64,2048]{2,1,0:T(8,128)(2,1)} copy(bf16[1,64,2048]{2,1,0:T(8,128)(2,1)} %bitcast.9) | data formatting | bytes 524288

commit v2 on v1

--- a/solution.py
+++ b/solution.py
@@ -302,10 +302,12 @@
 
         return first, second, last
 
-    for j, dest in enumerate(peers):
+    w_sends = []
+    for j in (0, 2, 1):
         for copy in stage_loads[j]:
             copy.wait()
-        send(remote(stage.at[j], w_view(s, f), w_s.at[j], w_r.at[s], z(dest)))
+        w_sends.append(remote(stage.at[j], w_view(s, f), w_s.at[j], w_r.at[s], z(peers[j])))
+        w_sends[-1].start()
     for j, dest in enumerate(peers):
         send(remote(spike, sbuf.at[s], sp_s.at[j], sp_r.at[s], z(dest)))
 
@@ -332,33 +334,52 @@
     x = tbuf[...].astype(F32)
     y = x * lax.rsqrt(jnp.mean(x * x, axis=-1, keepdims=True) + EPSILON) * gain_row
     nbuf[s, t] = y.astype(BF16)
-    for j, dest in enumerate((omid, mate)):
-        for c in range(CHUNKS):
-            view = tok_view(s, t, c)
-            send(remote(view, view, tz_s.at[j, c], tz_r.at[s, c], z(dest)))
+    to_mate = [
+        remote(tok_view(s, t, c), tok_view(s, t, c), tz_s.at[1, c], tz_r.at[s, c], z(mate)) for c in range(CHUNKS)
+    ]
+
+    @pl.when(is_mid)
+    def _():
+        for copy in to_mate:
+            copy.start()
+
     for c in range(CHUNKS):
         core_pass(s, c)
+    sbuf[s] = spike[...]
+
+    first, second, last = tree(w_view, wt_s, wt_r)
+
+    def w_arrival(j):
+        view = w_view(peers[j], f)
+        remote(view, view, w_s.at[j], w_r.at[peers[j]], z(peers[j])).wait_recv()
+
+    to_far = [
+        remote(tok_view(s, t, c), tok_view(s, t, c), tz_s.at[0, c], tz_r.at[s, c], z(omid)) for c in range(CHUNKS)
+    ]
+    w_arrival(0)
+    first(0, peers[0])
     for k, w_out in enumerate((w_po, w_ro)):
         dst = wo.at[k, ds(f * piece, piece), ds(lax.rem(s, 2) * cols, cols)]
         send(remote(w_out.at[ds(f * piece, piece), :], dst, wo_s.at[k], wo_r.at[k], z(mid)), is_end)
-    sbuf[s] = spike[...]
-
-    first, second, last = tree(w_view, wt_s, wt_r)
-
-    def w_arrival(j):
-        view = w_view(peers[j], f)
-        remote(view, view, w_s.at[j], w_r.at[peers[j]], z(peers[j])).wait_recv()
-
-    w_arrival(0)
-    first(0, peers[0])
     w_arrival(1)
     first(1, peers[1])
+
+    @pl.when(is_end)
+    def _():
+        for copy in to_far:
+            copy.start()
+        for copy in to_mate:
+            copy.start()
+
     second(0, peers[0])
-    w_arrival(2)
-    first(2, peers[2])
-    second(1, peers[1])
-    second(2, peers[2])
-
+
+    @pl.when(is_mid)
+    def _():
+        for copy in to_far:
+            copy.start()
+
+    for copy in to_mate + to_far + w_sends:
+        drains.append((None, copy))
     far = (omid, oend)
     relays = [
         [remote(tok_view(o, t, c), tok_view(o, t, c), tq_s.at[k, c], tz_r.at[o, c], z(end)) for c in range(CHUNKS)]
@@ -369,13 +390,37 @@
         for o in far
     ]
 
+    def relay(c):
+        for k, o in enumerate(far):
+            tok_arrival(o, c)
+            relays[k][c].start()
+            passes[k][c].start()
+
+    w_arrival(2)
+    first(2, peers[2])
+    pl.when(is_mid)(functools.partial(relay, 0))
+    second(1, peers[1])
+    pl.when(is_mid)(functools.partial(relay, 1))
+    second(2, peers[2])
+
     @pl.when(is_mid)
     def _():
-        for c in range(CHUNKS):
-            for k, o in enumerate(far):
-                tok_arrival(o, c)
-                relays[k][c].start()
-                passes[k][c].start()
+        for c in range(2, CHUNKS):
+            relay(c)
+
+    wo_first, wo_second, wo_last = tree(wo_view, ot_s, ot_r)
+    tree_from = len(drains)
+
+    @pl.when(is_mid)
+    def _():
+        for copy in late_loads[1:]:
+            copy.wait()
+        for k in range(2):
+            view = wo_view(k, f)
+            remote(view, view, wo_s.at[k], wo_r.at[k], z(end)).wait_recv()
+            mine = wo_view(k, f)
+            remote(mine, mine, ot_s.at[0, k], ot_r.at[0, k], at_x).start()
+            remote(mine, mine, ot_s.at[1, k], ot_r.at[1, k], at_y).start()
 
     for c in range(CHUNKS):
         tok_arrival(mate, c)
@@ -429,20 +474,6 @@
     counts = jnp.minimum(position + 1, window).astype(F32)
     pool_g[s] = (window_sum / counts - x).astype(BF16)
     send(remote(pool_g.at[s], pool_g.at[s], pg_s.at[0], pg_r.at[s], z(target)))
-
-    wo_first, wo_second, wo_last = tree(wo_view, ot_s, ot_r)
-    tree_from = len(drains)
-
-    @pl.when(is_mid)
-    def _():
-        for copy in late_loads[1:]:
-            copy.wait()
-        for k in range(2):
-            view = wo_view(k, f)
-            remote(view, view, wo_s.at[k], wo_r.at[k], z(end)).wait_recv()
-            mine = wo_view(k, f)
-            remote(mine, mine, ot_s.at[0, k], ot_r.at[0, k], at_x).start()
-            remote(mine, mine, ot_s.at[1, k], ot_r.at[1, k], at_y).start()
 
     for d in range(1, n_sp):
         o = lax.rem(s + d, n_sp)
@@ -508,12 +539,12 @@
 
     @pl.when(is_mid)
     def _():
-        pool_arrival(end)
-        pool_relay.start()
         for k in range(2):
             mark = len(drains)
             wo_second(k, k)
             del drains[mark:]
+        pool_arrival(end)
+        pool_relay.start()
         for i, p in enumerate(order):
             rec_arrival(end, p)
             rec_relays[i].start()
@@ -558,10 +589,13 @@
         view = obuf.at[side]
         remote(view, view, o_s.at[0], o_r.at[side], z(mid)).wait_recv()
 
+    def store(h):
+        return pltpu.make_async_copy(obuf.at[h], out.at[:, ds(2 * h * cols, 2 * cols)], ld.at[20 + h])
+
+    store(side).start()
     view = obuf.at[1 - side]
     remote(view, view, o_s.at[0], o_r.at[1 - side], z(omid)).wait_recv()
-    for h in range(2):
-        out[:, 2 * h * cols:2 * (h + 1) * cols] = obuf[h]
+    store(1 - side).start()
 
     for cond, copy in drains:
         if cond is None:
@@ -587,6 +621,9 @@
             on = wo_view(k, f_y, 1)
             remote(on, on, ot_s.at[3, k], ot_r.at[3, k], at_x).wait_send()
 
+    for h in range(2):
+        store(h).wait()
+
 
 def head_body(sizes, *args):
     (tokens, gain, w_pool, w_query, w_forget, w_value, maps, scale, low, spike, hgain, w_po, w_ro) = args
@@ -602,7 +639,7 @@
     here = pl.BlockSpec(memory_space=pl.ANY)
     result = pl.pallas_call(
         functools.partial(layer_kernel, n_fs, n_tp),
-        out_shape=jax.ShapeDtypeStruct((rows, n_sp * cols), BF16),
+        out_shape=pltpu.VMEM((rows, n_sp * cols), BF16),
         in_specs=[here, whole, here, here, here, here, here, whole, whole, whole, whole, here, here],
         out_specs=whole,
         scratch_shapes=[
@@ -621,7 +658,7 @@
             pltpu.VMEM((n_sp, rows, 2 * cols), BF16),
             pltpu.VMEM((n_sp, rows, 2 * cols), BF16),
             pltpu.VMEM((2, rows, 2 * cols), BF16),
-            dma((20,)),
+            dma((22,)),
             dma((3,)), dma((n_sp,)),
             dma((4, 3)), dma((4, 3)),
             dma((3,)), dma((n_sp,)),

time: 63.8 us -> 60.6 us (0.950)
  Pallas kernels: 62 us -> 59.7 us
  local copies, waits for them, and re-layouts: 1.67 us -> 0.71 us
    pallas_call x1, Pallas kernels: 62 us -> 59.7 us  [head_body(): pl.pallas_call(functools.partial(layer_kernel, n_fs, n_tp), out_shape=plt...]
    unnamed x1, local copies, waits for them, and re-layouts: 1.67 us -> 0.71 us
where the time goes in v2:
time: 60.6 us; the launch traced here: 60.4 us
  Pallas kernels  59.7 us (99%)
  local copies, waits for them, and re-layouts  0.71 us (1%)
    pallas_call x1, Pallas kernels, head_body(): pl.pallas_call(functools.partial(layer_kernel, n_fs, n_tp), out_shape=plt...  59.7 us

profile of v2, /device:TPU:0, one launch (start us, length us, event | category | flops | bytes accessed | tf_op | source)
XLA Modules:
  0.0 60.4 jit_solution(15220811364820255981)
XLA Ops:
  0.0 59.7 %layer.1 = bf16[64,2048]{1,0:T(8,128)(2,1)S(1)} custom-call(bf16[64,2048]{1,0:T(8,128)(2,1)} %bitcast.10, f32[1,2048]{1,0:T(1,128)} %bitcast.11, bf16[512,512]{1,0:T(8,128)(2,1)} %w_pool.1, bf16[512,512]{1,0:T(8,128)(2,1)} %w_query.1, bf16[512,512]{1,0:T(8,128)(2,1)} %w_forget.1, bf16[512,512]{1,0:T(8,128)(2,1)} %w_value.1, bf16[2,256,256]{2,1,0:T(8,128)(2,1)} %maps.1, ...), custom_call_target="tpu_custom_call" | custom-call | tf_op jit(solution)/shard_map/layer/pallas_call | solution.py:640
  59.7 0.7 %copy.15 = bf16[1,64,2048]{2,1,0:T(8,128)(2,1)} copy(bf16[1,64,2048]{2,1,0:T(8,128)(2,1)S(1)} %bitcast.9) | data formatting | bytes 524288

commit v3 on v1

v3 whole, which is shorter than its diff:
```python
import functools

import jax
import jax.numpy as jnp
from jax import lax
from jax.experimental import pallas as pl
from jax.experimental.pallas import tpu as pltpu
from jax.sharding import PartitionSpec as P

BLOCK = 64


EPSILON = 1e-06
HIGHEST = lax.Precision.HIGHEST


def shifted(value, axis, steps):
    count = lax.axis_size(axis)
    first, last = (max(0, -steps), min(count, count - steps))
    return lax.ppermute(value, axis, [(source, source + steps) for source in range(first, last)])


def entering(shard, axis, join, neutral):
    place = lax.axis_index(axis)
    gathered = jax.tree.map(
        lambda a, kind: lax.all_gather(a.astype(kind), axis), shard, (jnp.bfloat16, jnp.bfloat16)
    )
    state = jax.tree.map(lambda a, e: jnp.zeros_like(a) + jnp.asarray(e, a.dtype), shard, neutral)

    def one(step, state):
        return join(
            state,
            jax.tree.map(
                lambda a, own: lax.dynamic_index_in_dim(a, step, 0, False).astype(own.dtype),
                gathered,
                shard,
            ),
        )

    return lax.fori_loop(0, place, one, state)


def rms_scale(values, gain):
    return values * lax.rsqrt(jnp.mean(values * values, axis=-1, keepdims=True) + EPSILON) * gain


def join_state(earlier, later):
    decay_one, state_one = earlier
    decay_two, state_two = later
    return (decay_one * decay_two, decay_two[..., None] * state_one + state_two)


def body(
    tokens,
    input_norm_gain,
    pooling_input_weight,
    query_weight,
    forget_weight,
    value_weight,
    pooling_group_maps,
    pooling_scale,
    lower_bound_logits,
    decay_spike,
    head_norm_gain,
    pooling_output_weight,
    recurrent_output_weight,
):
    gathered = lax.all_gather(tokens, "tp", axis=1, tiled=True)[0]
    length_total = gathered.shape[0]
    normed = rms_scale(gathered.astype(jnp.float32), input_norm_gain).astype(jnp.bfloat16)
    pool_width = pooling_input_weight.shape[1]
    rec_width = query_weight.shape[1]
    stacked = jnp.concatenate(
        [pooling_input_weight, query_weight, forget_weight, value_weight], axis=1
    )
    out_local = jnp.concatenate([pooling_output_weight, recurrent_output_weight], axis=0)
    groups_fs = lax.axis_size("fs")
    member = lax.axis_index("fs")
    slice_width = stacked.shape[1] // groups_fs
    own_slice = lax.dynamic_slice_in_dim(stacked, member * slice_width, slice_width, 1)
    column_part = lax.all_gather(own_slice, "sp", axis=0, tiled=True)
    full_input = lax.all_gather(column_part, "fs", axis=1, tiled=True)
    projected = jnp.dot(normed, full_input, preferred_element_type=jnp.float32)
    slice_height = out_local.shape[0] // groups_fs
    own_rows = lax.dynamic_slice_in_dim(out_local, member * slice_height, slice_height, 0)
    row_part = lax.all_gather(own_rows, "sp", axis=1, tiled=True)
    out_full = lax.all_gather(row_part, "fs", axis=0, tiled=True)
    rounded = lax.optimization_barrier(projected.astype(jnp.bfloat16))
    pool_input = rounded[:, :pool_width]
    query_matrix = rounded[:, pool_width : pool_width + rec_width].astype(jnp.float32)
    forget_gate_logit = rounded[:, pool_width + rec_width : pool_width + 2 * rec_width].astype(
        jnp.float32
    )
    value_projected = rounded[:, pool_width + 2 * rec_width :].astype(jnp.float32)
    groups_local = pooling_group_maps.shape[0]
    group_size = pooling_group_maps.shape[1]
    reach_rows = 2 ** (groups_local * lax.axis_size("tp"))
    previous = shifted(pool_input[length_total - reach_rows :], "sp", 1)
    extended = jnp.concatenate([previous, pool_input], axis=0).astype(jnp.float32)
    extended = extended.reshape(reach_rows + length_total, groups_local, group_size)
    group_ids = lax.axis_index("tp") * groups_local + jnp.arange(groups_local, dtype=jnp.int32)
    windows = jnp.left_shift(jnp.int32(2), group_ids)
    window_sum = jnp.zeros((length_total, groups_local, group_size), jnp.float32)
    for offset in range(reach_rows):
        inside = (offset < windows).astype(jnp.float32)
        window_sum = (
            window_sum
            + extended[reach_rows - offset : reach_rows - offset + length_total] * inside[:, None]
        )
    position_index = lax.axis_index("sp") * length_total + jnp.arange(length_total, dtype=jnp.int32)
    counts = jnp.minimum(position_index[:, None] + 1, windows[None, :]).astype(jnp.float32)
    pool_diff = (window_sum / counts[:, :, None] - extended[reach_rows:]).astype(jnp.bfloat16)
    pool_mapped = jnp.einsum(
        "tgc,gcd->tgd", pool_diff, pooling_group_maps, preferred_element_type=jnp.float32
    )
    pool_out = (pool_mapped.reshape(length_total, pool_width) * pooling_scale).astype(jnp.bfloat16)
    local_heads = decay_spike.shape[2]
    head_width = rec_width // local_heads
    blocks = length_total // BLOCK
    block_layout = (blocks, BLOCK, local_heads, head_width)
    reader = jax.nn.silu(query_matrix).reshape(block_layout)
    key_gate_value = jax.nn.sigmoid(-lower_bound_logits) * jax.nn.sigmoid(-forget_gate_logit)
    decay_logarithm = (
        jnp.log1p(-key_gate_value).reshape(length_total, local_heads, head_width)
        + decay_spike[0][:, :, None]
    ).reshape(block_layout)
    key_rows = key_gate_value.reshape(block_layout)
    value_rows = value_projected.reshape(block_layout)
    inner_log = jnp.cumsum(decay_logarithm, axis=1)
    read_scaled = reader * jnp.exp(inner_log)
    key_scaled = key_rows * jnp.exp(-inner_log)
    causal = (jnp.arange(BLOCK)[:, None] >= jnp.arange(BLOCK)[None, :]).astype(jnp.float32)
    scores = jnp.einsum("nthd,nshd->nhts", read_scaled, key_scaled, precision=HIGHEST) * causal
    within = jnp.einsum("nhts,nshe->nthe", scores, value_rows, precision=HIGHEST)
    closing = inner_log[:, -1]
    key_tail = key_rows * jnp.exp(closing[:, None] - inner_log)
    deltas = jnp.einsum("nshd,nshe->nhde", key_tail, value_rows, precision=HIGHEST)
    block_decay = jnp.exp(closing)

    def advance(carried, input_batch):
        decay_now, delta_now = input_batch
        return (decay_now[..., None] * carried + delta_now, carried)

    initial = jnp.zeros((local_heads, head_width, head_width), jnp.float32)
    device_state, entry_states = lax.scan(advance, initial, (block_decay, deltas))
    device_decay = jnp.exp(jnp.sum(closing, axis=0))
    scanned = entering(
        (device_decay, device_state),
        "sp",
        join_state,
        (jnp.ones_like(device_decay), jnp.zeros_like(device_state)),
    )
    prior_state = scanned[1]
    before = jnp.cumsum(closing, axis=0) - closing
    start_states = entry_states + jnp.exp(before)[..., None] * prior_state[None]
    read_out = within + jnp.einsum("nthd,nhde->nthe", read_scaled, start_states, precision=HIGHEST)
    read_out = read_out.reshape(length_total, local_heads, head_width)
    recurrent_output = (
        rms_scale(read_out, 1.0).reshape(length_total, rec_width) * head_norm_gain
    ).astype(jnp.bfloat16)
    mixed_rows = jnp.concatenate([pool_out, recurrent_output], axis=1)
    summed = lax.psum_scatter(
        jnp.dot(mixed_rows, out_full, preferred_element_type=jnp.float32).astype(jnp.bfloat16),
        "tp",
        scatter_dimension=0,
        tiled=True,
    )
    return summed[None]


F32 = jnp.float32
BF16 = jnp.bfloat16
NT = (((1,), (1,)), ((), ()))
TN = (((0,), (0,)), ((), ()))

CHUNKS = 4


def layer_kernel(
    n_fs, n_tp,
    tok, gain, w_pool, w_query, w_forget, w_value, maps, scale, low, spike, hgain, w_po, w_ro,
    out,
    tbuf, stage, wbuf, nbuf, sbuf, proj, pool_g, rec_g, halo, wo, map_v, part, dbuf, summed, obuf,
    ld, w_s, w_r, wt_s, wt_r, sp_s, sp_r, tf_s, tm_s, tz_r, td_s, td_r,
    wo_s, wo_r, ot_s, ot_r, pg_s, pg_r, pq_s, h_s, h_r, rg_s, rg_r, d_s, d_r, o_s, o_r, gate,
):
    s = lax.axis_index("sp")
    f = lax.axis_index("fs")
    t = lax.axis_index("tp")
    n_sp = 4
    rows = tok.shape[0]
    depth = w_pool.shape[0]
    width = w_pool.shape[1] // n_sp
    cols = w_po.shape[1]
    piece = depth // n_fs
    half = piece // 2
    strip = n_tp * rows
    pair = 2 * width
    reach_rows = halo.shape[1]

    side = s // 2
    end, mid, omid, oend = 3 * side, 1 + side, 2 - side, 3 - 3 * side
    mate = end + mid - s
    is_end, is_mid = s == end, s == mid
    peers = (mate, omid, oend)
    positions = range(n_sp)
    far_side, own_side = 2 - 2 * side, 2 * side

    def z(o):
        return {"sp": o, "fs": f, "tp": t}

    at_x = {"sp": s, "fs": f + 1 - 2 * lax.rem(f, 2), "tp": t}
    at_y = {"sp": s, "fs": f + 2 - 4 * (f // 2), "tp": t}
    other = {"sp": s, "fs": f, "tp": 1 - t}
    f_x, f_y, f_d = at_x["fs"], at_y["fs"], 3 - f

    def ds(start, size):
        return pl.ds(pl.multiple_of(start, size), size)

    def remote(src, dst, ssem, rsem, dev):
        return pltpu.make_async_remote_copy(
            src_ref=src, dst_ref=dst, send_sem=ssem, recv_sem=rsem,
            device_id=dev, device_id_type=pl.DeviceIdType.MESH,
        )

    def moved(view, ssem, rsem, dev):
        return remote(view, view, ssem, rsem, dev)

    def when(cond, action):
        if cond is None:
            action()
        else:
            pl.when(cond)(action)

    def load(src, dst, i, cond=None):
        copy = pltpu.make_async_copy(src, dst, ld.at[i])
        when(cond, copy.start)
        return copy, cond

    def finish(loaded):
        when(loaded[1], loaded[0].wait)

    tok_load = load(tok, tbuf, 0)
    gates = (w_query, w_forget, w_value)
    stage_loads = []
    for j, dest in enumerate(peers):
        group_loads = []
        if j < 2:
            for m, w in enumerate(gates):
                group_loads.append(load(
                    w.at[ds(f * piece, piece), ds((dest // 2) * pair, pair)],
                    stage.at[j, :, pl.ds(m * pair, pair)], 1 + 4 * j + m, is_end if j == 0 else None,
                ))
        if j != 1:
            group_loads.append(load(
                w_pool.at[ds(f * piece, piece), :], stage.at[j, :, pl.ds(0, 2 * pair)],
                4 + 4 * j, is_mid if j == 0 else None,
            ))
        stage_loads.append(group_loads)
    own_rows = ds(s * depth, depth)
    own_loads = [
        load(w.at[:, ds(side * pair, pair)], wbuf.at[own_rows, pl.ds(m * pair, pair)], 13 + m, is_mid)
        for m, w in enumerate(gates)
    ]
    own_loads.append(load(w_pool, wbuf.at[own_rows, pl.ds(0, 2 * pair)], 16, is_end))
    map_load = load(maps, map_v, 17, is_end)
    wo_place = ds(lax.rem(s, 2) * cols, cols)
    wo_loads = [load(w, wo.at[k, :, wo_place], 18 + k, is_mid) for k, w in enumerate((w_po, w_ro))]

    barrier = pltpu.get_barrier_semaphore()
    partners = [z(o) for o in peers] + [at_x, at_y, other]
    for dev in partners:
        pl.semaphore_signal(barrier, inc=1, device_id=dev, device_id_type=pl.DeviceIdType.MESH)
    pl.semaphore_wait(barrier, len(partners))

    def w_send(j, span):
        dst = wbuf.at[ds(s * depth + f * piece, piece), pl.ds(0, span)]
        return remote(stage.at[j, :, pl.ds(0, span)], dst, w_s.at[j], w_r.at[s], z(peers[j]))

    to_mid_mate, to_end_mate = w_send(0, 3 * pair), w_send(0, 2 * pair)
    to_omid, to_oend = w_send(1, 3 * pair), w_send(2, 2 * pair)
    for j in (1, 0):
        for loaded in stage_loads[j]:
            finish(loaded)
    pl.when(is_mid)(to_omid.start)
    pl.when(is_mid)(to_end_mate.start)
    pl.when(is_end)(to_mid_mate.start)
    spike_sends = [remote(spike, sbuf.at[s], sp_s.at[j], sp_r.at[s], z(dest)) for j, dest in enumerate(peers)]
    for copy in spike_sends:
        copy.start()

    chunk = rows // CHUNKS

    def tok_view(o, core, c):
        return nbuf.at[o, core, pl.ds(c * chunk, chunk), :]

    def core_pass(o, c):
        return moved(tok_view(o, t, c), td_s.at[o, c], td_r.at[o, c], other)

    def core_arrival(o):
        for c in range(CHUNKS):
            moved(tok_view(o, 1 - t, c), td_s.at[o, c], td_r.at[o, c], other).wait_recv()

    finish(tok_load)
    x = tbuf[...].astype(F32)
    y = x * lax.rsqrt(jnp.mean(x * x, axis=-1, keepdims=True) + EPSILON) * gain[...]
    nbuf[s, t] = y.astype(BF16)
    to_mate = [moved(tok_view(s, t, c), tm_s.at[c], tz_r.at[s, c], z(mate)) for c in range(CHUNKS)]
    own_pass = [core_pass(s, c) for c in range(CHUNKS)]
    for copy in own_pass:
        copy.start()
    sbuf[s] = spike[...]
    finish(stage_loads[2][0])

    def tree(view, ssem, rsem, log):
        def start(copy):
            copy.start()
            log.append(copy)

        def first(i, o):
            start(moved(view(o, f), ssem.at[0, i], rsem.at[0, i], at_x))
            start(moved(view(o, f), ssem.at[1, i], rsem.at[1, i], at_y))

        def second(i, o):
            moved(view(o, f_x), ssem.at[0, i], rsem.at[0, i], at_x).wait_recv()
            start(moved(view(o, f_x, 0), ssem.at[2, i], rsem.at[2, i], at_y))
            moved(view(o, f_y), ssem.at[1, i], rsem.at[1, i], at_y).wait_recv()
            start(moved(view(o, f_y, 1), ssem.at[3, i], rsem.at[3, i], at_x))

        def last(i, o):
            moved(view(o, f_d, 0), ssem.at[2, i], rsem.at[2, i], at_y).wait_recv()
            moved(view(o, f_d, 1), ssem.at[3, i], rsem.at[3, i], at_x).wait_recv()

        return first, second, last

    def w_tree(span, log):
        def view(o, giver, h=None):
            start, size = o * depth + giver * piece, piece
            if h is not None:
                start, size = start + h * half, half
            return wbuf.at[ds(start, size), pl.ds(0, span)]

        def arrival(j):
            moved(view(peers[j], f), w_s.at[j], w_r.at[peers[j]], z(peers[j])).wait_recv()

        first, second, last = tree(view, wt_s, wt_r, log)
        return (
            arrival,
            lambda j: first(j, peers[j]),
            lambda j: second(j, peers[j]),
            lambda j: last(j, peers[j]),
        )

    def project(base, span):
        x = nbuf[pl.ds(base, 2)].reshape(2 * strip, nbuf.shape[3])
        y = jnp.dot(x, wbuf[:, :span], preferred_element_type=F32)
        proj[pl.ds(base, 2), :, :span] = y.astype(BF16).reshape(2, strip, span)

    def pool_view(p):
        return pool_g.at[ds(p * strip, strip), :]

    own_blocks = (own_side, own_side + 1)
    pool_sends = [moved(pool_view(p), pg_s.at[i], pg_r.at[p], z(mid)) for i, p in enumerate(own_blocks)]
    tok_arrivals = {
        o: [moved(tok_view(p, t, c), tm_s.at[c], tz_r.at[p, c], z(p)) for c in range(CHUNKS)]
        for o, p in (("mate", mate), ("omid", omid), ("oend", oend))
    }

    def store():
        for h in range(2):
            out[:, 2 * h * cols:2 * (h + 1) * cols] = obuf[h]

    def common_drains():
        for copy in spike_sends + own_pass:
            copy.wait_send()

    @pl.when(is_end)
    def _():
        log = []
        arrival, first, second, last = w_tree(2 * pair, log)
        to_mid_mate.wait_send()
        to_omid.start()
        arrival(0)
        first(0)
        to_omid.wait_send()
        to_oend.start()
        second(0)
        to_oend.wait_send()

        @pl.when(t == 0)
        def _():
            pl.semaphore_signal(gate, inc=1, device_id=other, device_id_type=pl.DeviceIdType.MESH)

        @pl.when(t == 1)
        def _():
            pl.semaphore_wait(gate, 1)

        for copy in to_mate:
            copy.start()
        arrival(1)
        first(1)
        arrival(2)
        first(2)
        for copy in to_mate:
            copy.wait_send()
        wo_sends = [
            remote(
                w.at[ds(f * piece, piece), :], wo.at[k, ds(f * piece, piece), wo_place], wo_s.at[k], wo_r.at[k], z(mid)
            )
            for k, w in enumerate((w_po, w_ro))
        ]
        for copy in wo_sends:
            copy.start()
        second(1)
        second(2)
        passes = [core_pass(mate, c) for c in range(CHUNKS)]
        for c in range(CHUNKS):
            tok_arrivals["mate"][c].wait_recv()
            passes[c].start()
        for j in range(3):
            last(j)
        finish(own_loads[3])
        core_arrival(s)
        core_arrival(mate)
        project(own_side, 2 * pair)
        halo_copy = remote(halo.at[0], halo.at[1], h_s.at[0], h_r.at[0], z(oend))

        @pl.when(side == 0)
        def _():
            halo[0] = proj[1, strip - reach_rows:, :2 * pair]
            halo_copy.start()
            halo[1] = jnp.zeros((reach_rows, 2 * pair), BF16)

        finish(map_load)
        groups = maps.shape[0]
        group = t * groups + lax.broadcasted_iota(jnp.int32, (strip, 2 * pair), 1) // pair
        position = lax.broadcasted_iota(jnp.int32, (strip, 2 * pair), 0)
        scale_row = scale[...]

        def pool(i, before):
            x = jnp.concatenate([before, proj[own_side + i, :, :2 * pair]], axis=0).astype(F32)
            total = x
            for g in range(n_tp * groups):
                reach = 2 ** g
                total = total + jnp.concatenate([jnp.zeros((reach, 2 * pair), F32), total[:-reach]], axis=0)
                if g == 0:
                    window_sum = total[reach_rows:]
                    window = jnp.full((strip, 2 * pair), 2, jnp.int32)
                else:
                    window_sum = jnp.where(group == g, total[reach_rows:], window_sum)
                    window = jnp.where(group == g, 2 ** (g + 1), window)
            counts = jnp.minimum((own_side + i) * strip + position + 1, window).astype(F32)
            diff = (window_sum / counts - x[reach_rows:]).astype(BF16)
            mapped = jnp.concatenate(
                [
                    jnp.dot(diff[:, g * pair:(g + 1) * pair], map_v[g], preferred_element_type=F32)
                    for g in range(groups)
                ],
                axis=1,
            )
            pool_g[ds((own_side + i) * strip, strip), :] = (mapped * scale_row).astype(BF16)

        pool(1, proj[own_side, strip - reach_rows:, :2 * pair])

        @pl.when(side == 1)
        def _():
            pool_sends[1].start()
            halo_copy.wait_recv()

        pool(0, halo[1])
        pool_sends[0].start()
        pl.when(side == 0)(pool_sends[1].start)
        for o in range(1, n_sp):
            origin = lax.rem(s + o, n_sp)
            remote(spike, sbuf.at[origin], sp_s.at[o - 1], sp_r.at[origin], z(origin)).wait_recv()
        common_drains()
        for copy in log + passes + wo_sends + pool_sends:
            copy.wait_send()
        pl.when(side == 0)(halo_copy.wait_send)
        moved(obuf.at[1 - side], o_s.at[0], o_r.at[1 - side], z(omid)).wait_recv()
        moved(obuf.at[side], o_s.at[0], o_r.at[side], z(mid)).wait_recv()
        store()

    @pl.when(is_mid)
    def _():
        log = []
        arrival, first, second, last = w_tree(3 * pair, log)
        to_far = [moved(tok_view(s, t, c), tf_s.at[0, c], tz_r.at[s, c], z(omid)) for c in range(CHUNKS)]
        relays = [moved(tok_view(mate, t, c), tf_s.at[1, c], tz_r.at[mate, c], z(omid)) for c in range(CHUNKS)]
        passes = {
            "mate": [core_pass(mate, c) for c in range(CHUNKS)],
            "omid": [core_pass(omid, c) for c in range(CHUNKS)],
            "oend": [core_pass(oend, c) for c in range(CHUNKS)],
        }

        def relay(c):
            tok_arrivals["mate"][c].wait_recv()
            relays[c].start()
            passes["mate"][c].start()

        def receive(o, c):
            tok_arrivals[o][c].wait_recv()
            passes[o][c].start()

        for copy in to_mate:
            copy.start()
        arrival(0)
        first(0)
        to_omid.wait_send()
        to_oend.start()
        arrival(1)
        first(1)
        second(0)
        arrival(2)
        first(2)
        to_oend.wait_send()

        @pl.when(t == 0)
        def _():
            pl.semaphore_signal(gate, inc=1, device_id=other, device_id_type=pl.DeviceIdType.MESH)

        @pl.when(t == 1)
        def _():
            pl.semaphore_wait(gate, 1)

        for copy in to_far:
            copy.start()
        second(1)
        relay(0)
        relay(1)
        relay(2)
        relay(3)
        second(2)
        for c in range(CHUNKS):
            receive("omid", c)
        def wo_view(k, giver, h=None):
            start, size = giver * piece, piece
            if h is not None:
                start, size = start + h * half, half
            return wo.at[k, ds(start, size), ds(lax.rem(end, 2) * cols, cols)]

        wo_first, wo_second, wo_last = tree(wo_view, ot_s, ot_r, log)
        for k in range(2):
            moved(wo_view(k, f), wo_s.at[k], wo_r.at[k], z(end)).wait_recv()
            wo_first(k, k)
        for c in range(CHUNKS):
            receive("oend", c)
        for j in range(3):
            last(j)
        for loaded in own_loads[:3]:
            finish(loaded)
        core_arrival(s)
        core_arrival(mate)
        project(own_side, 3 * pair)

        core_arrival(omid)
        core_arrival(oend)
        project(far_side, 3 * pair)

        def rec_view(o, p):
            return rec_g.at[o, ds(p * strip, strip), :]

        pool_relays = [moved(pool_view(p), pq_s.at[i], pg_r.at[p], z(omid)) for i, p in enumerate(own_blocks)]

        def pool_relay(i):
            pool_sends[i].wait_recv()
            pool_relays[i].start()

        rec_sends = [moved(rec_view(side, p), rg_s.at[p], rg_r.at[side, p], z(omid)) for p in positions]
        for d in range(1, n_sp):
            o = lax.rem(s + d, n_sp)
            remote(spike, sbuf.at[o], sp_s.at[d - 1], sp_r.at[o], z(o)).wait_recv()
        tri_r = lax.broadcasted_iota(jnp.int32, (BLOCK, BLOCK), 0)
        tri_c = lax.broadcasted_iota(jnp.int32, (BLOCK, BLOCK), 1)
        causal = tri_r >= tri_c
        tri = causal.astype(BF16)
        tri = jnp.concatenate([tri, tri, tri], axis=1)
        heads = range(pair // width)

        def per_head(values):
            return jnp.concatenate([values(2 * side + h) for h in heads], axis=1)

        gate_low = jax.nn.sigmoid(-per_head(lambda h: low[h]))
        head_gain = [hgain[2 * side + h] for h in heads]

        def column(o, h):
            row = jnp.broadcast_to(sbuf[o, pl.ds(2 * side + h, 1)], (8, strip))
            return jnp.broadcast_to(jnp.transpose(row)[:, :1], (strip, width))

        state = [jnp.zeros((width, width), F32) for h in heads]
        for p in positions:
            projected = proj[p]
            spikes = jnp.concatenate([column(p, h) for h in heads], axis=1)
            q = projected[:, :pair].astype(F32)
            reader = q * jax.nn.sigmoid(q)
            key = gate_low * jax.nn.sigmoid(-projected[:, pair:2 * pair].astype(F32))
            logs = jnp.log1p(-key) + spikes
            high = logs.astype(BF16)
            rest = logs - high.astype(F32)
            middle = rest.astype(BF16)
            lowest = (rest - middle.astype(F32)).astype(BF16)
            for b in range(strip // BLOCK):
                here = slice(b * BLOCK, (b + 1) * BLOCK)
                terms = jnp.concatenate([high[here], middle[here], lowest[here]], axis=0)
                inner = jnp.dot(tri, terms, preferred_element_type=F32)
                closing = inner[BLOCK - 1:]
                read_scaled = (reader[here] * jnp.exp(inner)).astype(BF16)
                key_scaled = (key[here] * jnp.exp(-inner)).astype(BF16)
                key_tail = (key[here] * jnp.exp(closing - inner)).astype(BF16)
                kept = jnp.exp(closing)
                for h in heads:
                    at = slice(h * width, (h + 1) * width)
                    v = projected[here, 2 * pair + h * width:2 * pair + (h + 1) * width]
                    scores = lax.dot_general(read_scaled[:, at], key_scaled[:, at], NT, preferred_element_type=F32)
                    scores = jnp.where(causal, scores, 0.0).astype(BF16)
                    read = jnp.dot(scores, v, preferred_element_type=F32)
                    read = read + lax.dot_general(
                        read_scaled[:, at], state[h].astype(BF16), NT, preferred_element_type=F32
                    )
                    state[h] = kept[:, at] * state[h] + lax.dot_general(
                        v, key_tail[:, at], TN, preferred_element_type=F32
                    )
                    rec = read * lax.rsqrt(jnp.mean(read * read, axis=-1, keepdims=True) + EPSILON) * head_gain[h]
                    rec_g[side, p * strip + b * BLOCK:p * strip + (b + 1) * BLOCK, at] = rec.astype(BF16)
            rec_sends[p].start()
            if p > 0 and p < 3:
                pl.when(side == 0)(functools.partial(pool_relay, p - 1))
            if p == 2:
                for k in range(2):
                    wo_second(k, k)

        for i in (1, 0):
            pl.when(side == 1)(functools.partial(pool_relay, i))
        for k in range(2):
            finish(wo_loads[k])
        for k in range(2):
            wo_last(k, k)
        w_full = wo[...].reshape(2 * wo.shape[1], wo.shape[2])
        blocks = (0, 1, 3, 2)

        def across(i):
            return remote(part.at[i, 1 - t], dbuf.at[i], d_s.at[i], d_r.at[i], other)

        def deliver(i):
            return remote(summed.at[i], obuf.at[side], o_s.at[i], o_r.at[side], z(blocks[i]))

        def settle(i):
            across(i).wait_recv()
            both = (part[i, t].astype(F32) + dbuf[i].astype(F32)).astype(BF16)

            @pl.when(s == blocks[i])
            def _():
                obuf[side] = both

            @pl.when(s != blocks[i])
            def _():
                summed[i] = both
                deliver(i).start()

        for i, p in enumerate(blocks):
            pl.when(side != p // 2)(moved(pool_view(p), pq_s.at[i // 2], pg_r.at[p], z(omid)).wait_recv)
            moved(rec_view(1 - side, p), rg_s.at[i], rg_r.at[1 - side, p], z(omid)).wait_recv()
            here = pl.ds(p * strip, strip)
            mixed = jnp.concatenate([pool_g[here, :], rec_g[0, here, :], rec_g[1, here, :]], axis=1)
            acc = jnp.dot(mixed, w_full, preferred_element_type=F32).astype(BF16)
            for core in range(n_tp):
                part[i, core] = acc[core * rows:(core + 1) * rows]
            across(i).start()
            if i > 0:
                settle(i - 1)
        settle(n_sp - 1)
        common_drains()
        for copy in log + to_mate + to_far + relays + passes["mate"] + passes["omid"] + passes["oend"]:
            copy.wait_send()
        for copy in rec_sends + pool_relays + [to_end_mate]:
            copy.wait_send()
        moved(obuf.at[1 - side], o_s.at[0], o_r.at[1 - side], z(omid)).wait_recv()
        store()
        for i in range(n_sp):
            across(i).wait_send()
            pl.when(s != blocks[i])(deliver(i).wait_send)


def head_body(sizes, *args):
    (tokens, gain, w_pool, w_query, w_forget, w_value, maps, scale, low, spike, hgain, w_po, w_ro) = args
    n_sp, n_fs, n_tp = sizes
    tok = tokens[0]
    rows, features = tok.shape
    depth = w_pool.shape[0]
    width = w_pool.shape[1] // n_sp
    length = n_sp * n_tp * rows
    cols = w_po.shape[1]
    dma = pltpu.SemaphoreType.DMA
    whole = pl.BlockSpec(memory_space=pltpu.VMEM)
    here = pl.BlockSpec(memory_space=pl.ANY)
    result = pl.pallas_call(
        functools.partial(layer_kernel, n_fs, n_tp),
        out_shape=pltpu.VMEM((rows, n_sp * cols), BF16),
        in_specs=[here, whole, here, here, here, here, here, whole, whole, whole, whole, here, here],
        out_specs=whole,
        scratch_shapes=[
            pltpu.VMEM((rows, features), BF16),
            pltpu.VMEM((3, depth // n_fs, 6 * width), BF16),
            pltpu.VMEM((features, 6 * width), BF16),
            pltpu.VMEM((n_sp, n_tp, rows, features), BF16),
            pltpu.VMEM((n_sp,) + (spike.shape[2], spike.shape[1]), F32),
            pltpu.VMEM((n_sp, n_tp * rows, 6 * width), BF16),
            pltpu.VMEM((length, 4 * width), BF16),
            pltpu.VMEM((2, length, 2 * width), BF16),
            pltpu.VMEM((2, 2 ** (n_tp * maps.shape[0]), 4 * width), BF16),
            pltpu.VMEM((2, w_po.shape[0], 2 * cols), BF16),
            pltpu.VMEM(maps.shape, BF16),
            pltpu.VMEM((n_sp, n_tp, rows, 2 * cols), BF16),
            pltpu.VMEM((n_sp, rows, 2 * cols), BF16),
            pltpu.VMEM((n_sp, rows, 2 * cols), BF16),
            pltpu.VMEM((2, rows, 2 * cols), BF16),
            dma((20,)),
            dma((3,)), dma((n_sp,)),
            dma((4, 3)), dma((4, 3)),
            dma((3,)), dma((n_sp,)),
            dma((2, CHUNKS)), dma((CHUNKS,)), dma((n_sp, CHUNKS)),
            dma((n_sp, CHUNKS)), dma((n_sp, CHUNKS)),
            dma((2,)), dma((2,)),
            dma((4, 2)), dma((4, 2)),
            dma((2,)), dma((n_sp,)), dma((2,)),
            dma((1,)), dma((1,)),
            dma((n_sp,)), dma((2, n_sp)),
            dma((n_sp,)), dma((n_sp,)),
            dma((n_sp,)), dma((2,)),
            pltpu.SemaphoreType.REGULAR,
        ],
        compiler_params=pltpu.CompilerParams(
            collective_id=0, has_side_effects=True, vmem_limit_bytes=56 * 1024 * 1024
        ),
        name="layer",
    )(
        tok, gain[None], w_pool, w_query, w_forget, w_value, maps, scale[None],
        low.reshape(n_sp, 1, width), spike[0].T, hgain.reshape(n_sp, 1, width), w_po, w_ro,
    )
    return result[None]


def solution(mesh):
    placed = (
        P("fs", ("sp", "tp"), None),
        P(),
        P("sp", "tp"),
        P("sp", "tp"),
        P("sp", "tp"),
        P("sp", "tp"),
        P("tp", None, None),
        P("tp"),
        P("tp"),
        P("fs", "sp", "tp"),
        P("tp"),
        P("tp", "sp"),
        P("tp", "sp"),
    )
    sizes = (mesh.shape["sp"], mesh.shape["fs"], mesh.shape["tp"])

    def one(*args):
        maps, spike = args[6], args[9]
        width = args[2].shape[1] // sizes[0]
        fits = spike.shape[2] == sizes[0] and sizes == (4, 4, 2) and width % 128 == 0
        fits = fits and args[3].shape[1] == args[2].shape[1] and maps.shape[:2] == (2, 2 * width)
        return head_body(sizes, *args) if fits else body(*args)

    return jax.shard_map(
        one, mesh=mesh, in_specs=placed, out_specs=P("fs", ("sp", "tp"), None), check_vma=False
    )
```

time: 63.8 us -> 58.2 us (0.912)
  Pallas kernels: 62 us -> 56.7 us
  local copies, waits for them, and re-layouts: 1.67 us -> 0.71 us
    pallas_call x1, Pallas kernels: 62 us -> 56.7 us  [head_body(): pl.pallas_call(functools.partial(layer_kernel, n_fs, n_tp), out_shape=plt...]
    unnamed x1, local copies, waits for them, and re-layouts: 1.67 us -> 0.71 us
where the time goes in v3:
time: 58.2 us; the launch traced here: 57.4 us
  Pallas kernels  56.7 us (97%)
  local copies, waits for them, and re-layouts  0.71 us (1%)
    pallas_call x1, Pallas kernels, head_body(): pl.pallas_call(functools.partial(layer_kernel, n_fs, n_tp), out_shape=plt...  56.7 us

profile of v3, /device:TPU:0, one launch (start us, length us, event | category | flops | bytes accessed | tf_op | source)
XLA Modules:
  0.0 57.4 jit_solution(18272245821372849328)
XLA Ops:
  0.0 56.7 %layer.1 = bf16[64,2048]{1,0:T(8,128)(2,1)S(1)} custom-call(bf16[64,2048]{1,0:T(8,128)(2,1)} %bitcast.10, f32[1,2048]{1,0:T(1,128)} %bitcast.11, bf16[512,512]{1,0:T(8,128)(2,1)} %w_pool.1, bf16[512,512]{1,0:T(8,128)(2,1)} %w_query.1, bf16[512,512]{1,0:T(8,128)(2,1)} %w_forget.1, bf16[512,512]{1,0:T(8,128)(2,1)} %w_value.1, bf16[2,256,256]{2,1,0:T(8,128)(2,1)} %maps.1, ...), custom_call_target="tpu_custom_call" | custom-call | tf_op jit(solution)/shard_map/layer/pallas_call | solution.py:696
  56.7 0.7 %copy.15 = bf16[1,64,2048]{2,1,0:T(8,128)(2,1)} copy(bf16[1,64,2048]{2,1,0:T(8,128)(2,1)S(1)} %bitcast.9) | data formatting | bytes 524288

commit v4 on v3

--- a/solution.py
+++ b/solution.py
@@ -240,6 +240,10 @@
     def finish(loaded):
         when(loaded[1], loaded[0].wait)
 
+    barrier = pltpu.get_barrier_semaphore()
+    partners = [z(o) for o in peers] + [at_x, at_y, other]
+    for dev in partners:
+        pl.semaphore_signal(barrier, inc=1, device_id=dev, device_id_type=pl.DeviceIdType.MESH)
     tok_load = load(tok, tbuf, 0)
     gates = (w_query, w_forget, w_value)
     stage_loads = []
@@ -267,10 +271,6 @@
     wo_place = ds(lax.rem(s, 2) * cols, cols)
     wo_loads = [load(w, wo.at[k, :, wo_place], 18 + k, is_mid) for k, w in enumerate((w_po, w_ro))]
 
-    barrier = pltpu.get_barrier_semaphore()
-    partners = [z(o) for o in peers] + [at_x, at_y, other]
-    for dev in partners:
-        pl.semaphore_signal(barrier, inc=1, device_id=dev, device_id_type=pl.DeviceIdType.MESH)
     pl.semaphore_wait(barrier, len(partners))
 
     def w_send(j, span):
@@ -279,10 +279,11 @@
 
     to_mid_mate, to_end_mate = w_send(0, 3 * pair), w_send(0, 2 * pair)
     to_omid, to_oend = w_send(1, 3 * pair), w_send(2, 2 * pair)
-    for j in (1, 0):
+    for j in (1, 0, 2):
         for loaded in stage_loads[j]:
             finish(loaded)
     pl.when(is_mid)(to_omid.start)
+    pl.when(is_mid)(to_oend.start)
     pl.when(is_mid)(to_end_mate.start)
     pl.when(is_end)(to_mid_mate.start)
     spike_sends = [remote(spike, sbuf.at[s], sp_s.at[j], sp_r.at[s], z(dest)) for j, dest in enumerate(peers)]
@@ -310,7 +311,6 @@
     for copy in own_pass:
         copy.start()
     sbuf[s] = spike[...]
-    finish(stage_loads[2][0])
 
     def tree(view, ssem, rsem, log):
         def start(copy):
@@ -506,25 +506,27 @@
             copy.start()
         arrival(0)
         first(0)
-        to_omid.wait_send()
-        to_oend.start()
         arrival(1)
         first(1)
+        to_omid.wait_send()
+        to_oend.wait_send()
+
+        @pl.when(t == 0)
+        def _():
+            pl.semaphore_signal(gate, inc=1, device_id=other, device_id_type=pl.DeviceIdType.MESH)
+            for copy in to_far:
+                copy.start()
+
         second(0)
         arrival(2)
         first(2)
-        to_oend.wait_send()
-
-        @pl.when(t == 0)
-        def _():
-            pl.semaphore_signal(gate, inc=1, device_id=other, device_id_type=pl.DeviceIdType.MESH)
 
         @pl.when(t == 1)
         def _():
             pl.semaphore_wait(gate, 1)
-
-        for copy in to_far:
-            copy.start()
+            for copy in to_far:
+                copy.start()
+
         second(1)
         relay(0)
         relay(1)
@@ -549,13 +551,20 @@
             last(j)
         for loaded in own_loads[:3]:
             finish(loaded)
-        core_arrival(s)
-        core_arrival(mate)
-        project(own_side, 3 * pair)
-
-        core_arrival(omid)
-        core_arrival(oend)
-        project(far_side, 3 * pair)
+
+        def tokens_of(first_side):
+            @pl.when(side == first_side)
+            def _():
+                core_arrival(s)
+                core_arrival(mate)
+
+            @pl.when(side != first_side)
+            def _():
+                core_arrival(omid)
+                core_arrival(oend)
+
+        tokens_of(0)
+        project(0, 3 * pair)
 
         def rec_view(o, p):
             return rec_g.at[o, ds(p * strip, strip), :]
@@ -589,6 +598,9 @@
 
         state = [jnp.zeros((width, width), F32) for h in heads]
         for p in positions:
+            if p == 2:
+                tokens_of(1)
+                project(2, 3 * pair)
             projected = proj[p]
             spikes = jnp.concatenate([column(p, h) for h in heads], axis=1)
             q = projected[:, :pair].astype(F32)
@@ -622,21 +634,31 @@
                     )
                     rec = read * lax.rsqrt(jnp.mean(read * read, axis=-1, keepdims=True) + EPSILON) * head_gain[h]
                     rec_g[side, p * strip + b * BLOCK:p * strip + (b + 1) * BLOCK, at] = rec.astype(BF16)
-            rec_sends[p].start()
+            if p == 1:
+                pl.when(side == 0)(rec_sends[p].start)
+            else:
+                rec_sends[p].start()
             if p > 0 and p < 3:
+                wo_second(p - 1, p - 1)
+            upper_one = jnp.logical_and(t == 1, side == 1)
+            upper_zero = jnp.logical_and(t == 0, side == 1)
+            if p == 0:
+                pl.when(upper_one)(functools.partial(pool_relay, 1))
+            if p == 1:
+                pl.when(upper_zero)(functools.partial(pool_relay, 1))
+            if p == 2:
+                pl.when(upper_one)(functools.partial(pool_relay, 0))
+            if p == 1 or p == 2:
                 pl.when(side == 0)(functools.partial(pool_relay, p - 1))
-            if p == 2:
-                for k in range(2):
-                    wo_second(k, k)
-
-        for i in (1, 0):
-            pl.when(side == 1)(functools.partial(pool_relay, i))
+        pl.when(jnp.logical_and(t == 0, side == 1))(functools.partial(pool_relay, 0))
+        pl.when(side == 1)(rec_sends[1].start)
         for k in range(2):
             finish(wo_loads[k])
         for k in range(2):
             wo_last(k, k)
         w_full = wo[...].reshape(2 * wo.shape[1], wo.shape[2])
-        blocks = (0, 1, 3, 2)
+        blocks = (0 * side, 3 - 2 * side, 2 + side, 1 + side)
+        crossed = (side == 1, None, side == 0)
 
         def across(i):
             return remote(part.at[i, 1 - t], dbuf.at[i], d_s.at[i], d_r.at[i], other)
@@ -658,9 +680,10 @@
                 deliver(i).start()
 
         for i, p in enumerate(blocks):
-            pl.when(side != p // 2)(moved(pool_view(p), pq_s.at[i // 2], pg_r.at[p], z(omid)).wait_recv)
+            if i < 3:
+                when(crossed[i], moved(pool_view(p), pq_s.at[0], pg_r.at[p], z(omid)).wait_recv)
             moved(rec_view(1 - side, p), rg_s.at[i], rg_r.at[1 - side, p], z(omid)).wait_recv()
-            here = pl.ds(p * strip, strip)
+            here = ds(p * strip, strip)
             mixed = jnp.concatenate([pool_g[here, :], rec_g[0, here, :], rec_g[1, here, :]], axis=1)
             acc = jnp.dot(mixed, w_full, preferred_element_type=F32).astype(BF16)
             for core in range(n_tp):

time: 58.2 us -> 57.3 us (0.985)
  Pallas kernels: 56.7 us -> 55.6 us
    pallas_call x1, Pallas kernels: 56.7 us -> 55.6 us  [head_body(): pl.pallas_call(functools.partial(layer_kernel, n_fs, n_tp), out_shape=plt...]
where the time goes in v4:
time: 57.3 us; the launch traced here: 56.4 us
  Pallas kernels  55.6 us (97%)
  local copies, waits for them, and re-layouts  0.71 us (1%)
    pallas_call x1, Pallas kernels, head_body(): pl.pallas_call(functools.partial(layer_kernel, n_fs, n_tp), out_shape=plt...  55.6 us

profile of v4, /device:TPU:0, one launch (start us, length us, event | category | flops | bytes accessed | tf_op | source)
XLA Modules:
  0.0 56.4 jit_solution(4367484730687262440)
XLA Ops:
  0.0 55.6 %layer.1 = bf16[64,2048]{1,0:T(8,128)(2,1)S(1)} custom-call(bf16[64,2048]{1,0:T(8,128)(2,1)} %bitcast.10, f32[1,2048]{1,0:T(1,128)} %bitcast.11, bf16[512,512]{1,0:T(8,128)(2,1)} %w_pool.1, bf16[512,512]{1,0:T(8,128)(2,1)} %w_query.1, bf16[512,512]{1,0:T(8,128)(2,1)} %w_forget.1, bf16[512,512]{1,0:T(8,128)(2,1)} %w_value.1, bf16[2,256,256]{2,1,0:T(8,128)(2,1)} %maps.1, ...), custom_call_target="tpu_custom_call" | custom-call | tf_op jit(solution)/shard_map/layer/pallas_call | solution.py:719
  55.7 0.7 %copy.15 = bf16[1,64,2048]{2,1,0:T(8,128)(2,1)} copy(bf16[1,64,2048]{2,1,0:T(8,128)(2,1)S(1)} %bitcast.9) | data formatting | bytes 524288

commit v5 on v4

--- a/solution.py
+++ b/solution.py
@@ -173,7 +173,7 @@
 NT = (((1,), (1,)), ((), ()))
 TN = (((0,), (0,)), ((), ()))
 
-CHUNKS = 4
+CHUNKS = 2
 
 
 def layer_kernel(
@@ -384,19 +384,9 @@
         first(0)
         to_omid.wait_send()
         to_oend.start()
-        second(0)
-        to_oend.wait_send()
-
-        @pl.when(t == 0)
-        def _():
-            pl.semaphore_signal(gate, inc=1, device_id=other, device_id_type=pl.DeviceIdType.MESH)
-
-        @pl.when(t == 1)
-        def _():
-            pl.semaphore_wait(gate, 1)
-
         for copy in to_mate:
             copy.start()
+        second(0)
         arrival(1)
         first(1)
         arrival(2)
@@ -474,7 +464,7 @@
             origin = lax.rem(s + o, n_sp)
             remote(spike, sbuf.at[origin], sp_s.at[o - 1], sp_r.at[origin], z(origin)).wait_recv()
         common_drains()
-        for copy in log + passes + wo_sends + pool_sends:
+        for copy in log + passes + wo_sends + pool_sends + [to_oend]:
             copy.wait_send()
         pl.when(side == 0)(halo_copy.wait_send)
         moved(obuf.at[1 - side], o_s.at[0], o_r.at[1 - side], z(omid)).wait_recv()
@@ -509,7 +499,6 @@
         arrival(1)
         first(1)
         to_omid.wait_send()
-        to_oend.wait_send()
 
         @pl.when(t == 0)
         def _():
@@ -530,8 +519,6 @@
         second(1)
         relay(0)
         relay(1)
-        relay(2)
-        relay(3)
         second(2)
         for c in range(CHUNKS):
             receive("omid", c)
@@ -689,13 +676,11 @@
             for core in range(n_tp):
                 part[i, core] = acc[core * rows:(core + 1) * rows]
             across(i).start()
-            if i > 0:
-                settle(i - 1)
-        settle(n_sp - 1)
+            settle(i)
         common_drains()
         for copy in log + to_mate + to_far + relays + passes["mate"] + passes["omid"] + passes["oend"]:
             copy.wait_send()
-        for copy in rec_sends + pool_relays + [to_end_mate]:
+        for copy in rec_sends + pool_relays + [to_end_mate, to_oend]:
             copy.wait_send()
         moved(obuf.at[1 - side], o_s.at[0], o_r.at[1 - side], z(omid)).wait_recv()
         store()

time: 57.3 us -> 55.6 us (0.970); the launches traced: 56.4 us -> 55.4 us
  Pallas kernels: 55.6 us -> 54.7 us
    pallas_call x1, Pallas kernels: 55.6 us -> 54.7 us  [head_body(): pl.pallas_call(functools.partial(layer_kernel, n_fs, n_tp), out_shape=plt...]
where the time goes in v5:
time: 55.6 us; the launch traced here: 55.4 us
  Pallas kernels  54.7 us (98%)
  local copies, waits for them, and re-layouts  0.71 us (1%)
    pallas_call x1, Pallas kernels, head_body(): pl.pallas_call(functools.partial(layer_kernel, n_fs, n_tp), out_shape=plt...  54.7 us

profile of v5, /device:TPU:0, one launch (start us, length us, event | category | flops | bytes accessed | tf_op | source)
XLA Modules:
  0.0 55.4 jit_solution(1547150392489494164)
XLA Ops:
  0.0 54.7 %layer.1 = bf16[64,2048]{1,0:T(8,128)(2,1)S(1)} custom-call(bf16[64,2048]{1,0:T(8,128)(2,1)} %bitcast.10, f32[1,2048]{1,0:T(1,128)} %bitcast.11, bf16[512,512]{1,0:T(8,128)(2,1)} %w_pool.1, bf16[512,512]{1,0:T(8,128)(2,1)} %w_query.1, bf16[512,512]{1,0:T(8,128)(2,1)} %w_forget.1, bf16[512,512]{1,0:T(8,128)(2,1)} %w_value.1, bf16[2,256,256]{2,1,0:T(8,128)(2,1)} %maps.1, ...), custom_call_target="tpu_custom_call" | custom-call | tf_op jit(solution)/shard_map/layer/pallas_call | solution.py:704
  54.7 0.7 %copy.15 = bf16[1,64,2048]{2,1,0:T(8,128)(2,1)} copy(bf16[1,64,2048]{2,1,0:T(8,128)(2,1)S(1)} %bitcast.9) | data formatting | bytes 524288

commit v6 on v5

--- a/solution.py
+++ b/solution.py
@@ -366,9 +366,8 @@
         for o, p in (("mate", mate), ("omid", omid), ("oend", oend))
     }
 
-    def store():
-        for h in range(2):
-            out[:, 2 * h * cols:2 * (h + 1) * cols] = obuf[h]
+    def store(h):
+        out[:, ds(2 * h * cols, 2 * cols)] = obuf[h]
 
     def common_drains():
         for copy in spike_sends + own_pass:
@@ -468,8 +467,9 @@
             copy.wait_send()
         pl.when(side == 0)(halo_copy.wait_send)
         moved(obuf.at[1 - side], o_s.at[0], o_r.at[1 - side], z(omid)).wait_recv()
+        store(1 - side)
         moved(obuf.at[side], o_s.at[0], o_r.at[side], z(mid)).wait_recv()
-        store()
+        store(side)
 
     @pl.when(is_mid)
     def _():
@@ -682,8 +682,9 @@
             copy.wait_send()
         for copy in rec_sends + pool_relays + [to_end_mate, to_oend]:
             copy.wait_send()
+        store(side)
         moved(obuf.at[1 - side], o_s.at[0], o_r.at[1 - side], z(omid)).wait_recv()
-        store()
+        store(1 - side)
         for i in range(n_sp):
             across(i).wait_send()
             pl.when(s != blocks[i])(deliver(i).wait_send)

time: 55.6 us -> 55.6 us (level)
  no operation moved by 1% of the time
where the time goes in v6:
time: 55.6 us; the launch traced here: 55.4 us
  Pallas kernels  54.7 us (98%)
  local copies, waits for them, and re-layouts  0.71 us (1%)
    pallas_call x1, Pallas kernels, head_body(): pl.pallas_call(functools.partial(layer_kernel, n_fs, n_tp), out_shape=plt...  54.7 us

profile of v6, /device:TPU:0, one launch (start us, length us, event | category | flops | bytes accessed | tf_op | source)
XLA Modules:
  0.0 55.4 jit_solution(5966438042474223558)
XLA Ops:
  0.0 54.7 %layer.1 = bf16[64,2048]{1,0:T(8,128)(2,1)S(1)} custom-call(bf16[64,2048]{1,0:T(8,128)(2,1)} %bitcast.10, f32[1,2048]{1,0:T(1,128)} %bitcast.11, bf16[512,512]{1,0:T(8,128)(2,1)} %w_pool.1, bf16[512,512]{1,0:T(8,128)(2,1)} %w_query.1, bf16[512,512]{1,0:T(8,128)(2,1)} %w_forget.1, bf16[512,512]{1,0:T(8,128)(2,1)} %w_value.1, bf16[2,256,256]{2,1,0:T(8,128)(2,1)} %maps.1, ...), custom_call_target="tpu_custom_call" | custom-call | tf_op jit(solution)/shard_map/layer/pallas_call | solution.py:705
  54.7 0.7 %copy.15 = bf16[1,64,2048]{2,1,0:T(8,128)(2,1)} copy(bf16[1,64,2048]{2,1,0:T(8,128)(2,1)S(1)} %bitcast.9) | data formatting | bytes 524288
